TPU v7x, 256 devices: a whole 4x4x8 slice. The times are simulated.
256 devices in a mesh: ra: 32 (over z, y), cb: 8 (over x, core).
Axes of the slice: x: 4, y: 4, z: 8, core: 2. Of those that a mesh axis runs over, the one named last changes fastest.
Arguments:
- stream: bfloat16 [64, 1024], P(None, 'ra'), may hold values from -24 to 24, as said below
- gain_first: float32 [1024], P('ra'), may hold values from 0.5 to 1.5
- up_first: float32 [1024, 4096], P('ra', 'cb'), may hold values from -0.1875 to 0.1875
- down_first: float32 [4096, 1024], P('cb', 'ra'), may hold values from -0.09375 to 0.09375
- gain_second: float32 [1024], P('ra'), may hold values from 0.5 to 1.5
- up_second: float32 [1024, 4096], P('ra', 'cb'), may hold values from -0.1875 to 0.1875
- down_second: float32 [4096, 1024], P('cb', 'ra'), may hold values from -0.09375 to 0.09375
Outputs:
- read: bfloat16 [64, 1024], P(None, 'ra')
Inputs may be any that keep to these rules, and one draw needn't show every extreme that they name: stream is of order one, and in each token one aligned block of 32 features is four times larger than the rest.
All inputs are finite; a program needn't handle non-finite values.
Results may differ from a plain program's by a relative error of at most 0.025.
Values may be sent and summed in bfloat16 or wider, within the bound.
A program may use at most 64 MiB of HBM per device.

v0:
```python
import jax
import jax.numpy as jnp
from jax import lax
from jax.sharding import Mesh
from jax.sharding import PartitionSpec as P

D = 1024
RA = ("ra_0", "ra_1")


EPS = 1e-06
RESIDUAL = 0.25


def by_axis(array, axes):
    for axis in axes:
        array = lax.psum(array, axis)
    return array


def total_of_pieces(array, axis):
    pieces = lax.all_gather(array, axis)
    return pieces.sum(axis=0)


def over_pieces(array, axis):
    return lax.all_gather(array, axis).astype(jnp.float32).sum(0)


def sublayer(stream, norm_gain, w_up, w_down):
    floated = stream.astype(jnp.float32)
    own_squares = jnp.sum(floated * floated, axis=1, keepdims=True)
    squares = by_axis(own_squares, RA)
    factor = lax.rsqrt(squares / D + EPS)
    normed = (floated * factor * norm_gain.astype(jnp.float32)[None, :]).astype(jnp.bfloat16)
    up_bf = w_up.astype(jnp.bfloat16)
    down_bf = w_down.astype(jnp.bfloat16)
    partial_value = jnp.dot(normed, up_bf, preferred_element_type=jnp.float32)
    preact = total_of_pieces(partial_value, RA)
    activated = jnp.square(jax.nn.relu(preact)).astype(jnp.bfloat16)
    down_part = jnp.dot(activated, down_bf, preferred_element_type=jnp.float32)
    branch = over_pieces(down_part.astype(jnp.bfloat16), "cb").astype(jnp.float32)
    return (RESIDUAL * floated + branch).astype(jnp.bfloat16)


def local(stream, gain_first, up_first, down_first, gain_second, up_second, down_second):
    middle = sublayer(stream, gain_first, up_first, down_first)
    return sublayer(middle, gain_second, up_second, down_second)


def solution(mesh):
    torus = Mesh(mesh.devices.reshape(8, 4, mesh.shape["cb"]), ("ra_0", "ra_1", "cb"))
    in_specs = (P(None, RA), P(RA), P(RA, "cb"), P("cb", RA), P(RA), P(RA, "cb"), P("cb", RA))
    out_specs = P(None, RA)
    return jax.shard_map(local, mesh=torus, in_specs=in_specs, out_specs=out_specs, check_vma=False)
```

profile of v0, /device:TPU:1, one launch (start us, length us, event | category | flops | bytes accessed | tf_op | source)
XLA Modules:
  0.0 262.1 jit_solution(6546073855465038196)
XLA Ops:
  6.5 0.0 copy-start
  6.5 0.0 copy-start.1
  6.5 0.0 copy-start.2
  6.5 0.0 copy-start.4
  6.5 0.0 all-gather.9.cloned.1.call-start
  6.6 0.8 fusion.12
  7.3 17.3 %psum.28 = f32[64,1]{0,1:T(1,128)S(1)} all-reduce(f32[64,1]{0,1:T(1,128)S(1)} %bitcast.15), channel_id=1, replica_groups=mesh['ra_0'=8,'ra_1'=4,'cb'=8] {'ra_0'}, use_global_device_ids=true, to_apply=%region_1.0 | all-reduce | flops 64 | bytes 512 | tf_op jit(solution)/shard_map/psum | solution.py:17
  24.6 8.7 %psum.29 = f32[64,1]{0,1:T(1,128)S(1)} all-reduce(f32[64,1]{0,1:T(1,128)S(1)} %psum.28), channel_id=1, replica_groups=mesh['ra_0'=8,'ra_1'=4,'cb'=8] {'ra_1'}, use_global_device_ids=true, to_apply=%region_2.0 | all-reduce | flops 64 | bytes 512 | tf_op jit(solution)/shard_map/psum | solution.py:17
  33.4 1.8 fusion.8
  35.1 0.0 all-gather.9.cloned.1.call-update
  35.2 0.0 all-gather.11.cloned.1.call-start
  35.2 79.5 %all-gather.9.cloned.1.call-done = f32[2048,512]{1,0:T(8,128)} async-done(((f32[64,512]{1,0:T(8,128)}), f32[2048,512]{1,0:T(8,128)}) %all-gather.9.cloned.1.call-update) | async-done | bytes 4194320 | tf_op jit(solution)/shard_map/all_gather | solution.py:22
  114.7 0.0 copy-start.3
  114.7 2.6 reduce_sum.55
  117.3 0.0 copy-done.1
  117.3 0.1 fusion
  117.4 17.4 %all-gather.4 = bf16[8,64,32]{1,2,0:T(8,128)(2,1)S(1)} all-gather(bf16[1,64,32]{1,2,0:T(8,128)(2,1)S(1)} %fusion), channel_id=3, replica_groups=mesh['ra_0'=8,'ra_1'=4,'cb'=8] {'cb'}, dimensions={0}, use_global_device_ids=true | all-gather | bytes 36864 | tf_op jit(solution)/shard_map/all_gather | solution.py:27
  134.8 0.0 copy-done
  134.9 12.3 %psum.30 = f32[64,1]{0,1:T(1,128)S(1)} all-reduce(f32[64,1]{0,1:T(1,128)S(1)} %bitcast.14), channel_id=1, replica_groups=mesh['ra_0'=8,'ra_1'=4,'cb'=8] {'ra_0'}, use_global_device_ids=true, to_apply=%region_6.7 | all-reduce | flops 64 | bytes 512 | tf_op jit(solution)/shard_map/psum | solution.py:17
  147.2 6.5 %psum.31 = f32[64,1]{0,1:T(1,128)S(1)} all-reduce(f32[64,1]{0,1:T(1,128)S(1)} %psum.30), channel_id=1, replica_groups=mesh['ra_0'=8,'ra_1'=4,'cb'=8] {'ra_1'}, use_global_device_ids=true, to_apply=%region_7.8 | all-reduce | flops 64 | bytes 512 | tf_op jit(solution)/shard_map/psum | solution.py:17
  153.7 0.0 copy-done.2
  153.7 0.0 copy-done.4
  153.7 0.9 fusion.5
  154.7 0.0 all-gather.11.cloned.1.call-update
  154.7 79.9 %all-gather.11.cloned.1.call-done = f32[2048,512]{1,0:T(8,128)} async-done(((f32[64,512]{1,0:T(8,128)}), f32[2048,512]{1,0:T(8,128)}) %all-gather.11.cloned.1.call-update) | async-done | bytes 4194320 | tf_op jit(solution)/shard_map/all_gather | solution.py:22
  234.6 2.5 reduce_sum.58
  237.1 0.0 copy-done.3
  237.1 0.1 fusion.1
  237.2 17.4 %all-gather.5 = bf16[8,64,32]{1,2,0:T(8,128)(2,1)S(1)} all-gather(bf16[1,64,32]{1,2,0:T(8,128)(2,1)S(1)} %fusion.1), channel_id=5, replica_groups=mesh['ra_0'=8,'ra_1'=4,'cb'=8] {'cb'}, dimensions={0}, use_global_device_ids=true | all-gather | bytes 36864 | tf_op jit(solution)/shard_map/all_gather | solution.py:27
  254.6 0.6 fusion.16
  (5 shorter events, 0.1 us)
Async XLA Ops:
  6.5 128.3 %copy-start = (bf16[64,32]{0,1:T(8,128)(2,1)S(1)}, bf16[64,32]{0,1:T(8,128)(2,1)}, u32[]{:S(2)}) copy-start(bf16[64,32]{0,1:T(8,128)(2,1)} %param.7) | copy-start | bytes 12292
  6.5 110.8 %copy-start.1 = (f32[512,32]{0,1:T(8,128)S(1)}, f32[512,32]{0,1:T(8,128)}, u32[]{:S(2)}) copy-start(f32[512,32]{0,1:T(8,128)} %param.10) | copy-start | bytes 196612
  6.5 147.2 %copy-start.2 = (f32[32,512]{1,0:T(8,128)S(1)}, f32[32,512]{1,0:T(8,128)}, u32[]{:S(2)}) copy-start(f32[32,512]{1,0:T(8,128)} %param.12) | copy-start | bytes 196612
  6.5 147.2 %copy-start.4 = (f32[32]{0:T(128)S(1)}, f32[32]{0:T(128)}, u32[]{:S(2)}) copy-start(f32[32]{0:T(128)} %param.11) | copy-start | bytes 388
  6.5 108.2 %all-gather.9.cloned.1.call-start = ((), (), s32[]{:S(2)}) async-start(), calls=%async_computation | async-start | bytes 4325376 | tf_op jit(solution)/shard_map/all_gather | solution.py:22
  35.2 199.4 %all-gather.11.cloned.1.call-start = ((), (), s32[]{:S(2)}) async-start(), calls=%async_computation.1 | async-start | bytes 4325376 | tf_op jit(solution)/shard_map/all_gather | solution.py:22
  114.7 122.4 %copy-start.3 = (f32[512,32]{0,1:T(8,128)S(1)}, f32[512,32]{0,1:T(8,128)}, u32[]{:S(2)}) copy-start(f32[512,32]{0,1:T(8,128)} %param.13) | copy-start | bytes 196612
Sparse Core Ops, SparseCore 0:
  35.3 79.3 all-gather.8
  154.8 79.7 all-gather.10
where the time goes:
time: 262 us
  waiting for transfers between devices  159 us (61%)
  blocking collectives  79.6 us (30%)
  between operations  13.4 us (5%)
  other arithmetic  6.52 us (2%)
  matrix products  2.96 us (1%)
    all_gather x2, waiting for transfers between devices, total_of_pieces(): pieces = lax.all_gather(array, axis)  159 us
    psum x4, blocking collectives, by_axis(): array = lax.psum(array, axis)  44.9 us
    all_gather x2, blocking collectives, over_pieces(): return lax.all_gather(array, axis).astype(jnp.float32).sum(0)  34.7 us
  transfers between devices with their start and end apart: 2, of which 2 were waited for; matrix products, arithmetic and copies ran while one was open for 0% of the time, Pallas kernels for 0%

commit v1 on v0

v1 whole, which is shorter than its diff:
```python
import jax
import jax.numpy as jnp
from jax import lax
from jax.experimental import pallas as pl
from jax.experimental.pallas import tpu as pltpu
from jax.sharding import PartitionSpec as P

D = 1024
EPS = 1e-06
RESIDUAL = 0.25
RA, CB = 32, 8
HALF = 64


def block_diagonal(packed, left):
    rolled = pltpu.roll(packed, HALF, 1)
    zero = jnp.zeros_like(packed)
    return jnp.concatenate(
        [
            jnp.where(left, packed, zero),
            jnp.where(left, rolled, zero),
            jnp.where(left, zero, rolled),
            jnp.where(left, zero, packed),
        ],
        axis=0,
    )


def kernel(
    stream_hbm, gain_a, up_a, down_a, gain_b, up_b, down_b, out_ref,
    stream_v, gain_v, up_v, down_v, upt_v, part_send, part_recv, act_send, act_recv, x_send, x_recv,
    load_sem, part_ss, part_rs, act_ss, act_rs, x_ss, x_rs,
):
    me = lax.axis_index("ra")
    col = lax.axis_index("cb")
    barrier = pltpu.get_barrier_semaphore()

    @pl.loop(1, RA)
    def _(step):
        pl.semaphore_signal(barrier, inc=1, device_id={"ra": lax.rem(me + step, RA)})

    @pl.loop(1, CB)
    def _(step):
        pl.semaphore_signal(barrier, inc=1, device_id={"cb": lax.rem(col + step, CB)})

    loads = [
        pltpu.make_async_copy(stream_hbm, stream_v, load_sem.at[0]),
        pltpu.make_async_copy(gain_a, gain_v.at[0], load_sem.at[1]),
        pltpu.make_async_copy(up_a, up_v.at[0], load_sem.at[2]),
        pltpu.make_async_copy(down_a, down_v.at[0], load_sem.at[3]),
        pltpu.make_async_copy(gain_b, gain_v.at[1], load_sem.at[4]),
        pltpu.make_async_copy(up_b, up_v.at[1], load_sem.at[5]),
        pltpu.make_async_copy(down_b, down_v.at[1], load_sem.at[6]),
    ]
    for load in loads:
        load.start()

    left = lax.broadcasted_iota(jnp.int32, (16, 128), 1) < HALF

    def prepare_up(layer):
        rows = up_v[layer].astype(jnp.bfloat16).astype(jnp.float32)
        stacked = jnp.concatenate([rows[:, :256], rows[:, 256:]], axis=0)
        gain = gain_v[layer]
        gains = jnp.concatenate([gain, gain], axis=1)
        upt_v[layer] = (stacked.T * gains).astype(jnp.bfloat16)

    def up_partial(layer, packed):
        blocks = block_diagonal(packed, left)
        squares = jnp.sum(blocks * blocks, axis=0, keepdims=True)
        high = squares.astype(jnp.bfloat16)
        low = (squares - high.astype(jnp.float32)).astype(jnp.bfloat16)
        pair = jnp.where(
            lax.broadcasted_iota(jnp.int32, (8, 128), 0) < 4,
            jnp.broadcast_to(high.astype(jnp.float32), (8, 128)),
            jnp.broadcast_to(low.astype(jnp.float32), (8, 128)),
        )
        partial = jnp.dot(upt_v[layer], blocks.astype(jnp.bfloat16), preferred_element_type=jnp.float32)
        tiles = jnp.concatenate(
            [partial.reshape(RA, 8, 128), jnp.broadcast_to(pair[None], (RA, 8, 128))], axis=1
        )
        part_send[layer] = tiles.astype(jnp.bfloat16)

    loads[0].wait()
    loads[1].wait()
    loads[2].wait()
    prepare_up(0)
    u_left = stream_v[...].astype(jnp.float32)
    u_both = jnp.concatenate([u_left, u_left], axis=1)
    packed = jnp.where(left, u_both[:16], u_both[16:])
    up_partial(0, packed)

    for layer in range(2):
        if layer == 0:
            pl.semaphore_wait(barrier, RA - 1 + CB - 1)
        part_recv[layer, me] = part_send[layer, me]

        @pl.loop(1, RA)
        def _(step):
            other = lax.rem(me + step, RA)
            pltpu.make_async_remote_copy(
                src_ref=part_send.at[layer, other],
                dst_ref=part_recv.at[layer, me],
                send_sem=part_ss.at[layer],
                recv_sem=part_rs.at[layer],
                device_id={"ra": other},
            ).start()

        if layer == 0:
            for load in loads[3:]:
                load.wait()
            prepare_up(1)
        down = down_v[layer].astype(jnp.bfloat16)
        down = jnp.concatenate([down[:, :256], down[:, 256:]], axis=0)

        arrived = part_recv.at[layer, pl.ds(0, RA - 1)]
        pltpu.make_async_copy(arrived, arrived, part_rs.at[layer]).wait()
        total = jnp.sum(part_recv[layer].astype(jnp.float32), axis=0)
        squares = total[8:9] + total[12:13]
        factor = lax.rsqrt(squares / D + EPS)
        preact = total[:8] * factor
        act_send[layer] = jnp.square(jnp.maximum(preact, 0.0)).astype(jnp.bfloat16)
        act_recv[layer, me] = act_send[layer]

        @pl.loop(1, RA)
        def _(step):
            other = lax.rem(me + step, RA)
            pltpu.make_async_remote_copy(
                src_ref=act_send.at[layer],
                dst_ref=act_recv.at[layer, me],
                send_sem=act_ss.at[layer],
                recv_sem=act_rs.at[layer],
                device_id={"ra": other},
            ).start()

        arrived = act_recv.at[layer, pl.ds(0, RA - 1)]
        pltpu.make_async_copy(arrived, arrived, act_rs.at[layer]).wait()
        activated = act_recv[layer].astype(jnp.float32).reshape(256, 128).astype(jnp.bfloat16)
        both = jnp.dot(down, activated, preferred_element_type=jnp.float32)
        straight = jnp.where(left, both[:16], both[48:])
        crossed = jnp.where(left, both[16:32], both[32:48])
        branch = straight + pltpu.roll(crossed, HALF, 1)
        x_send[layer] = branch.astype(jnp.bfloat16)
        x_recv[layer, col] = x_send[layer]

        @pl.loop(1, CB)
        def _(step):
            other = lax.rem(col + step, CB)
            pltpu.make_async_remote_copy(
                src_ref=x_send.at[layer],
                dst_ref=x_recv.at[layer, col],
                send_sem=x_ss.at[layer],
                recv_sem=x_rs.at[layer],
                device_id={"cb": other},
            ).start()

        arrived = x_recv.at[layer, pl.ds(0, CB - 1)]
        pltpu.make_async_copy(arrived, arrived, x_rs.at[layer]).wait()
        summed = jnp.sum(x_recv[layer].astype(jnp.float32), axis=0)
        packed = (RESIDUAL * packed + summed).astype(jnp.bfloat16).astype(jnp.float32)
        if layer == 0:
            up_partial(1, packed)

    rolled = pltpu.roll(packed, HALF, 1)
    result = jnp.concatenate([packed, rolled], axis=0)
    out_ref[...] = result[:, :HALF].astype(jnp.bfloat16)

    for layer in range(2):
        sent = part_recv.at[layer, pl.ds(0, RA - 1)]
        pltpu.make_async_copy(sent, sent, part_ss.at[layer]).wait()
        sent = act_recv.at[layer, pl.ds(0, RA - 1)]
        pltpu.make_async_copy(sent, sent, act_ss.at[layer]).wait()
        sent = x_recv.at[layer, pl.ds(0, CB - 1)]
        pltpu.make_async_copy(sent, sent, x_ss.at[layer]).wait()


def local(stream, gain_first, up_first, down_first, gain_second, up_second, down_second):
    call = pl.pallas_call(
        kernel,
        out_shape=jax.ShapeDtypeStruct((32, 64), jnp.bfloat16),
        in_specs=[pl.BlockSpec(memory_space=pl.ANY)] * 7,
        out_specs=pl.BlockSpec(memory_space=pltpu.VMEM),
        scratch_shapes=[
            pltpu.VMEM((32, 64), jnp.bfloat16),
            pltpu.VMEM((2, 1, 32), jnp.float32),
            pltpu.VMEM((2, 32, 512), jnp.float32),
            pltpu.VMEM((2, 32, 512), jnp.float32),
            pltpu.VMEM((2, 256, 64), jnp.bfloat16),
            pltpu.VMEM((2, RA, 16, 128), jnp.bfloat16),
            pltpu.VMEM((2, RA, 16, 128), jnp.bfloat16),
            pltpu.VMEM((2, 8, 128), jnp.bfloat16),
            pltpu.VMEM((2, RA, 8, 128), jnp.bfloat16),
            pltpu.VMEM((2, 16, 128), jnp.bfloat16),
            pltpu.VMEM((2, CB, 16, 128), jnp.bfloat16),
            pltpu.SemaphoreType.DMA((7,)),
        ]
        + [pltpu.SemaphoreType.DMA((2,))] * 6,
        compiler_params=pltpu.CompilerParams(collective_id=0, has_side_effects=True),
    )
    out = call(
        stream.T, gain_first[None], up_first, down_first.T, gain_second[None], up_second, down_second.T
    )
    return out.T


def solution(mesh):
    in_specs = (P(None, "ra"), P("ra"), P("ra", "cb"), P("cb", "ra"), P("ra"), P("ra", "cb"), P("cb", "ra"))
    return jax.shard_map(local, mesh=mesh, in_specs=in_specs, out_specs=P(None, "ra"), check_vma=False)
```

time: 262 us -> 48.4 us (0.18)
  waiting for transfers between devices: 159 us -> 0 us
  blocking collectives: 79.6 us -> 0 us
  Pallas kernels: 0 us -> 46.9 us
  between operations: 13.4 us -> 0.01 us
  other arithmetic: 6.52 us -> 0 us
  matrix products: 2.96 us -> 0 us
    all_gather x2 -> x0, waiting for transfers between devices: 159 us -> none  [total_of_pieces(): pieces = lax.all_gather(array, axis)]
    pallas_call x0 -> x1, Pallas kernels: none -> 46.9 us  [local(): call(stream.T, gain_first[None], up_first, down_first.T, gain_second[None...]
    psum x4 -> x0, blocking collectives: 44.9 us -> none  [by_axis(): array = lax.psum(array, axis)]
    all_gather x2 -> x0, blocking collectives: 34.7 us -> none  [over_pieces(): return lax.all_gather(array, axis).astype(jnp.float32).sum(0)]
    reduce_sum x6 -> x0, other arithmetic: 5.9 us -> none  [the longest x2 5.09 us: total_of_pieces(): return pieces.sum(axis=0)]
    dot_general x4 -> x0, matrix products: 2.96 us -> none  [the longest x2 2.69 us: sublayer(): partial_value = jnp.dot(normed, up_bf, preferred_element_type=jnp.float32)]
  transfers between devices with their start and end apart: 2 -> 0, of which waited for: 2 -> 0; matrix products, arithmetic and copies ran while one was open for 0% -> 0% of each run, Pallas kernels for 0% -> 0%
where the time goes in v1:
time: 48.4 us; the launch traced here: 48.2 us
  Pallas kernels  46.9 us (97%)
  local copies, waits for them, and re-layouts  1.3 us (3%)
    pallas_call x1, Pallas kernels, local(): call(stream.T, gain_first[None], up_first, down_first.T, gain_second[None...  46.9 us
    unnamed x1, local copies, waits for them, and re-layouts  1.3 us

profile of v1, /device:TPU:1, one launch (start us, length us, event | category | flops | bytes accessed | tf_op | source)
XLA Modules:
  0.0 48.2 jit_solution(6841791727351033757)
XLA Ops:
  0.0 46.9 %shard_map.73 = bf16[32,64]{1,0:T(8,128)(2,1)} custom-call(bf16[32,64]{1,0:T(8,128)(2,1)} %bitcast.9, f32[1,32]{1,0:T(1,128)} %bitcast.10, f32[32,512]{1,0:T(8,128)} %up_a.1, f32[32,512]{1,0:T(8,128)} %bitcast.6, f32[1,32]{1,0:T(1,128)} %bitcast.11, f32[32,512]{1,0:T(8,128)} %up_b.1, f32[32,512]{1,0:T(8,128)} %bitcast.7), custom_call_target="tpu_custom_call" | custom-call | tf_op jit(solution)/shard_map/pallas_call | solution.py:199
  46.9 1.3 %copy.9 = bf16[64,32]{0,1:T(8,128)(2,1)} copy(bf16[64,32]{0,1:T(8,128)(2,1)} %bitcast.8) | data formatting | bytes 8192

commit v2 on v0

v2 whole, which is shorter than its diff:
```python
import jax
import jax.numpy as jnp
from jax import lax
from jax.experimental import pallas as pl
from jax.experimental.pallas import tpu as pltpu
from jax.sharding import PartitionSpec as P

D = 1024
EPS = 1e-06
RESIDUAL = 0.25
BF = jnp.bfloat16
F32 = jnp.float32


def nt(a, b):
    return lax.dot_general(a, b, (((1,), (1,)), ((), ())), preferred_element_type=F32)


def nn(a, b):
    return jnp.dot(a, b, preferred_element_type=F32)


def lanes(shape):
    return lax.broadcasted_iota(jnp.int32, shape, len(shape) - 1)


def packed_of(both):
    return jnp.where(lanes((16, 128)) < 64, both[:16], both[16:])


def kernel(
    stream_h, gain_a, up_a, down_a, gain_b, up_b, down_b, out_ref,
    stream_v, gain_v, up_v, down_v,
    up1, down1s, up2s, down2,
    ps, pr, ys, yr, down1, up2y, up2, xs, xr, ms, mr, acts, actr, fs, fr, rs, rr,
    load_sem, give_ss, give_rs, ps_s, pr_s, ys_s, yr_s, d1_ss, d1_rs, u1_ss, u1_rs, u2_ss, u2_rs,
    xs_s, xr_s, ms_s, mr_s, as_s, ar_s, fs_s, fr_s, rs_s, rr_s,
):
    ra, cb = lax.axis_index("ra"), lax.axis_index("cb")
    z, y = ra // 4, ra % 4
    x, c = cb // 2, cb % 2
    barrier = pltpu.get_barrier_semaphore()
    loads = [
        pltpu.make_async_copy(src, dst, load_sem.at[k])
        for k, (src, dst) in enumerate(
            [
                (stream_h, stream_v),
                (gain_a, gain_v.at[0]),
                (up_a, up_v.at[0]),
                (down_a, down_v.at[0]),
                (gain_b, gain_v.at[1]),
                (up_b, up_v.at[1]),
                (down_b, down_v.at[1]),
            ]
        )
    ]

    def at(dz, dy, dx, core):
        return {"ra": ((z + dz) % 8) * 4 + (y + dy) % 4, "cb": ((x + dx) % 4) * 2 + core}

    def send(src, dst, ss, rsem, where):
        pltpu.make_async_remote_copy(
            src_ref=src, dst_ref=dst, send_sem=ss, recv_sem=rsem, device_id=where
        ).start()

    def drain(ref, sem):
        pltpu.make_async_copy(ref, ref, sem).wait()

    def hello(where):
        pl.semaphore_signal(barrier, inc=1, device_id=where)

    def prepare_up1():
        up1[c] = up_v[0].astype(BF)

    def prepare_down1():
        down1s[c] = down_v[0].astype(BF)

    def prepare_up2():
        eye = lax.broadcasted_iota(jnp.int32, (32, 32), 0) == lanes((32, 32))
        column = jnp.sum(jnp.where(eye, gain_v[1], 0.0), axis=1, keepdims=True)
        scaled = (up_v[1].astype(BF).astype(F32) * column).astype(BF)
        for k in range(4):
            up2s[k, c] = scaled[:, 128 * k : 128 * k + 128]

    def prepare_down2():
        down2[c] = down_v[1].astype(BF)

    def finish():
        total = jnp.sum(fr[...].astype(F32), axis=0) + rr[...]
        total = total.astype(BF).astype(F32)
        rolled = pltpu.roll(total, 64, 1)
        out_ref[...] = jnp.concatenate([total, rolled], axis=0)[:, :64].astype(BF)

    @pl.when(c == 0)
    def _():
        for dx in range(4):
            hello(at(0, 0, dx, 1))
        for load in loads[2:]:
            load.start()
        loads[2].wait()
        prepare_up1()
        pl.semaphore_wait(barrier, 1)
        partner = at(0, 0, 0, 1)
        send(up1.at[0], up1.at[0], give_ss.at[0], give_rs.at[0], partner)
        loads[3].wait()
        prepare_down1()
        send(down1s.at[0], down1s.at[0], give_ss.at[1], give_rs.at[1], partner)
        loads[4].wait()
        loads[5].wait()
        prepare_up2()
        send(up2s.at[:, 0], up2s.at[:, 0], give_ss.at[2], give_rs.at[2], partner)
        loads[6].wait()
        prepare_down2()
        send(down2.at[0], down2.at[0], give_ss.at[3], give_rs.at[3], partner)
        drain(up1.at[0], give_ss.at[0])
        drain(down1s.at[0], give_ss.at[1])
        drain(up2s.at[:, 0], give_ss.at[2])
        drain(down2.at[0], give_ss.at[3])
        drain(rr, rr_s)
        drain(fr, fr_s)
        finish()

    @pl.when(c == 1)
    def _():
        far = (4, 3, 5, 2, 6, 1, 7)
        for dz in far:
            hello(at(dz, 0, 0, 1))
        for d in (2, 1, 3):
            hello(at(0, d, 0, 1))
            hello(at(0, 0, d, 1))
        hello(at(0, 0, 0, 0))
        for load in loads:
            load.start()

        for k in range(2):
            loads[k].wait()
        u = stream_v[...].astype(F32).T
        place = lanes((32, 128)) == 32 * (z % 4) + lax.broadcasted_iota(jnp.int32, (32, 128), 0)
        tile = nn(u.astype(BF), place.astype(F32).astype(BF))
        ps[:, :, 1024:] = tile.reshape(8, 8, 128).astype(BF)
        lhs = (u * gain_v[0]).astype(BF)
        loads[2].wait()
        prepare_up1()
        ps[:, :, 512:1024] = nn(lhs, up1[1]).reshape(8, 8, 512).astype(BF)
        drain(up1.at[0], give_rs.at[0])
        ps[:, :, :512] = nn(lhs, up1[0]).reshape(8, 8, 512).astype(BF)

        pl.semaphore_wait(barrier, 17)
        for dz in far:
            send(ps.at[(z + dz) % 8], pr.at[z], ps_s, pr_s, at(dz, 0, 0, 1))
        pr[z] = ps[z]
        loads[3].wait()
        prepare_down1()
        for dz in far:
            send(down1s.at[1], down1.at[1, z], d1_ss, d1_rs, at(dz, 0, 0, 1))
        loads[4].wait()
        loads[5].wait()
        prepare_up2()
        drain(up2s.at[:, 0], give_rs.at[2])
        for dy in (2, 1, 3):
            send(up2s.at[(y + dy) % 4], up2y.at[y], u1_ss, u1_rs, at(0, dy, 0, 1))
        drain(down1s.at[0], give_rs.at[1])
        for dz in far:
            send(down1s.at[0], down1.at[0, z], d1_ss, d1_rs, at(dz, 0, 0, 1))
        up2y[y] = up2s[y]
        down1[0, z] = down1s[0]
        down1[1, z] = down1s[1]

        drain(pr.at[pl.ds(0, 7)], pr_s)
        partial = jnp.sum(pr[:, :, :1024].astype(F32), axis=0)
        u_own = jnp.concatenate(
            [
                jnp.sum(pr[0:4, :, 1024:].astype(F32), axis=0),
                jnp.sum(pr[4:8, :, 1024:].astype(F32), axis=0),
            ],
            axis=1,
        )
        squares = jnp.sum(u_own * u_own, axis=1, keepdims=True)
        high = squares.astype(BF).astype(F32)
        ys[:, :1024] = partial.astype(BF)
        ys[:, 1024:] = jnp.where(lanes((8, 128)) < 64, high, squares - high).astype(BF)
        for dy in (2, 1, 3):
            send(ys, yr.at[y], ys_s, yr_s, at(0, dy, 0, 1))
        yr[y] = ys[...]

        drain(up2y.at[pl.ds(0, 3)], u1_rs)
        for dz in far:
            send(up2y, up2.at[z], u2_ss, u2_rs, at(dz, 0, 0, 1))
        up2[z] = up2y[...]

        drain(yr.at[pl.ds(0, 3)], yr_s)
        preact = jnp.sum(yr[...].astype(F32), axis=0)
        squares = jnp.sum(preact[:, 1024:], axis=1, keepdims=True) / 64
        factor = lax.rsqrt(squares / D + EPS)
        act = jnp.square(jnp.maximum(preact[:, :1024] * factor, 0.0)).astype(BF)

        drain(down1.at[:, pl.ds(0, 7)], d1_rs)
        branch = nt(act[:, :512], down1[0].reshape(256, 512)) + nt(act[:, 512:], down1[1].reshape(256, 512))
        share = jnp.where(x == 0, RESIDUAL, 0.0)
        xs[...] = (branch + share * u_own).astype(BF)
        for dy in (2, 1, 3, 0):
            for dx in (2, 1, 3, 0):
                if dy or dx:
                    send(xs, xr.at[4 * y + x], xs_s, xr_s, at(0, dy, dx, 1))
        xr[4 * y + x] = xs[...]
        loads[6].wait()
        prepare_down2()
        drain(down2.at[0], give_rs.at[3])

        drain(xr.at[pl.ds(0, 15)], xr_s)
        middle = jnp.sum(xr[...].astype(F32).reshape(4, 4, 8, 256), axis=1).astype(BF).astype(F32)
        middle = jnp.concatenate([middle[k] for k in range(4)], axis=1)
        squares = jnp.sum(middle * middle, axis=1, keepdims=True)
        factor = lax.rsqrt(squares / D + EPS)
        middle = middle.astype(BF)
        drain(up2.at[pl.ds(0, 7)], u2_rs)
        pre = []
        for k in range(2):
            rows = jnp.concatenate([up2[a, b, k] for b in range(4) for a in range(8)], axis=0)
            pre.append(nn(middle, rows))
        act = jnp.square(jnp.maximum(jnp.concatenate(pre, axis=1) * factor, 0.0))
        acts[...] = act.astype(BF)

        @pl.loop(1, 32)
        def _(step):
            send(acts, actr.at[8 * y + z], as_s, ar_s, at(step // 4, step % 4, 0, 1))

        actr[8 * y + z] = acts[...]
        own = jnp.sum(xr[pl.ds(4 * y, 4)].astype(F32), axis=0).astype(BF)
        ms[0] = own[:, :128]
        ms[1] = own[:, 128:]
        for dz in far:
            send(ms.at[((z + dz) % 8) // 4], mr.at[z], ms_s, mr_s, at(dz, 0, 0, 1))
        mr[z] = ms[z // 4]
        drain(mr.at[pl.ds(0, 7)], mr_s)
        mid = mr[...].astype(F32).reshape(64, 128).astype(BF)
        mid = jnp.concatenate([mid, mid], axis=0)
        rs[...] = RESIDUAL * packed_of(nt(place.astype(F32).astype(BF), mid))
        send(rs, rr, rs_s, rr_s, at(0, 0, 0, 0))
        rr[...] = rs[...]

        drain(actr.at[pl.ds(0, 31)], ar_s)
        weights = jnp.concatenate(
            [down2[k, :, 128 * b : 128 * b + 128] for b in range(4) for k in range(2)], axis=1
        )
        gathered = actr[...].astype(F32).reshape(4, 64, 256)
        gathered = jnp.concatenate([gathered[b] for b in range(4)], axis=1).astype(BF)
        gathered = jnp.concatenate([gathered, gathered], axis=0)
        fs[...] = packed_of(nt(weights, gathered)).astype(BF)
        for dx in (2, 1, 3):
            send(fs, fr.at[x], fs_s, fr_s, at(0, 0, dx, 0))
            send(fs, fr.at[x], fs_s, fr_s, at(0, 0, dx, 1))
        send(fs, fr.at[x], fs_s, fr_s, at(0, 0, 0, 0))
        fr[x] = fs[...]
        drain(fr.at[pl.ds(0, 3)], fr_s)
        finish()

        drain(ps.at[pl.ds(0, 7)], ps_s)
        drain(down1.at[:, pl.ds(0, 7)], d1_ss)
        drain(up2y.at[pl.ds(0, 3)], u1_ss)
        drain(yr.at[pl.ds(0, 3)], ys_s)
        drain(up2.at[pl.ds(0, 7)], u2_ss)
        drain(xr.at[pl.ds(0, 15)], xs_s)
        drain(actr.at[pl.ds(0, 31)], as_s)
        drain(mr.at[pl.ds(0, 7)], ms_s)
        drain(rr, rs_s)
        drain(xr.at[pl.ds(0, 7)], fs_s)


def local(stream, gain_first, up_first, down_first, gain_second, up_second, down_second):
    vmem = [
        ((32, 64), BF), ((2, 1, 32), F32), ((2, 32, 512), F32), ((2, 32, 512), F32),
        ((2, 32, 512), BF), ((2, 32, 512), BF), ((4, 2, 32, 128), BF), ((2, 32, 512), BF),
        ((8, 8, 1152), BF), ((8, 8, 1152), BF), ((8, 1152), BF), ((4, 8, 1152), BF),
        ((2, 8, 32, 512), BF), ((4, 2, 32, 128), BF), ((8, 4, 2, 32, 128), BF),
        ((8, 256), BF), ((16, 8, 256), BF), ((2, 8, 128), BF), ((8, 8, 128), BF),
        ((8, 256), BF), ((32, 8, 256), BF), ((16, 128), BF), ((4, 16, 128), BF),
        ((16, 128), F32), ((16, 128), F32),
    ]
    dma = pltpu.SemaphoreType.DMA
    call = pl.pallas_call(
        kernel,
        out_shape=jax.ShapeDtypeStruct((32, 64), BF),
        in_specs=[pl.BlockSpec(memory_space=pl.ANY)] * 7,
        out_specs=pl.BlockSpec(memory_space=pltpu.VMEM),
        scratch_shapes=[pltpu.VMEM(*v) for v in vmem] + [dma((7,)), dma((4,)), dma((4,))] + [dma(())] * 20,
        compiler_params=pltpu.CompilerParams(collective_id=0, has_side_effects=True),
    )
    out = call(
        stream.T, gain_first[None], up_first, down_first.T, gain_second[None], up_second, down_second.T
    )
    return out.T


def solution(mesh):
    in_specs = (P(None, "ra"), P("ra"), P("ra", "cb"), P("cb", "ra"), P("ra"), P("ra", "cb"), P("cb", "ra"))
    return jax.shard_map(local, mesh=mesh, in_specs=in_specs, out_specs=P(None, "ra"), check_vma=False)
```

time: 262 us -> 37.5 us (0.14)
  waiting for transfers between devices: 159 us -> 0 us
  blocking collectives: 79.6 us -> 0 us
  Pallas kernels: 0 us -> 36 us
  between operations: 13.4 us -> 0.01 us
  other arithmetic: 6.52 us -> 0 us
  matrix products: 2.96 us -> 0 us
    all_gather x2 -> x0, waiting for transfers between devices: 159 us -> none  [total_of_pieces(): pieces = lax.all_gather(array, axis)]
    psum x4 -> x0, blocking collectives: 44.9 us -> none  [by_axis(): array = lax.psum(array, axis)]
    pallas_call x0 -> x1, Pallas kernels: none -> 36 us  [local(): call(stream.T, gain_first[None], up_first, down_first.T, gain_second[None...]
    all_gather x2 -> x0, blocking collectives: 34.7 us -> none  [over_pieces(): return lax.all_gather(array, axis).astype(jnp.float32).sum(0)]
    reduce_sum x6 -> x0, other arithmetic: 5.9 us -> none  [the longest x2 5.09 us: total_of_pieces(): return pieces.sum(axis=0)]
    dot_general x4 -> x0, matrix products: 2.96 us -> none  [the longest x2 2.69 us: sublayer(): partial_value = jnp.dot(normed, up_bf, preferred_element_type=jnp.float32)]
  transfers between devices with their start and end apart: 2 -> 0, of which waited for: 2 -> 0; matrix products, arithmetic and copies ran while one was open for 0% -> 0% of each run, Pallas kernels for 0% -> 0%
where the time goes in v2:
time: 37.5 us; the launch traced here: 37.3 us
  Pallas kernels  36 us (96%)
  local copies, waits for them, and re-layouts  1.3 us (3%)
    pallas_call x1, Pallas kernels, local(): call(stream.T, gain_first[None], up_first, down_first.T, gain_second[None...  36 us
    unnamed x1, local copies, waits for them, and re-layouts  1.3 us

profile of v2, /device:TPU:1, one launch (start us, length us, event | category | flops | bytes accessed | tf_op | source)
XLA Modules:
  0.0 37.3 jit_solution(8906045945703023639)
XLA Ops:
  0.0 36.0 %shard_map.73 = bf16[32,64]{1,0:T(8,128)(2,1)} custom-call(bf16[32,64]{1,0:T(8,128)(2,1)} %bitcast.9, f32[1,32]{1,0:T(1,128)} %bitcast.10, f32[32,512]{1,0:T(8,128)} %up_a.1, f32[32,512]{1,0:T(8,128)} %bitcast.6, f32[1,32]{1,0:T(1,128)} %bitcast.11, f32[32,512]{1,0:T(8,128)} %up_b.1, f32[32,512]{1,0:T(8,128)} %bitcast.7), custom_call_target="tpu_custom_call" | custom-call | tf_op jit(solution)/shard_map/pallas_call | solution.py:289
  36.0 1.3 %copy.9 = bf16[64,32]{0,1:T(8,128)(2,1)} copy(bf16[64,32]{0,1:T(8,128)(2,1)} %bitcast.8) | data formatting | bytes 8192

commit v3 on v2

v3 whole, which is shorter than its diff:
```python
import jax
import jax.numpy as jnp
from jax import lax
from jax.experimental import pallas as pl
from jax.experimental.pallas import tpu as pltpu
from jax.sharding import PartitionSpec as P

D = 1024
EPS = 1e-06
RESIDUAL = 0.25
BF = jnp.bfloat16
F32 = jnp.float32


def nt(a, b):
    return lax.dot_general(a, b, (((1,), (1,)), ((), ())), preferred_element_type=F32)


def nn(a, b):
    return jnp.dot(a, b, preferred_element_type=F32)


def lanes(shape):
    return lax.broadcasted_iota(jnp.int32, shape, len(shape) - 1)


def packed_of(both):
    return jnp.where(lanes((16, 128)) < 64, both[:16], both[16:])


def kernel(
    stream_h, gain_a, up_a, down_a, gain_b, up_b, down_b, out_ref,
    stream_v, gain_v, up_v, down_v,
    down1s, up2s, down2,
    ps, pr0, pr1, ys, yr, down1, up2y, up2, xs, xr, ms, mr, acts, actr, fs, fr, rs, rr,
    load_sem, give_ss, give_rs, ps_s, pr0_s, pr1_s, ys_s, yr_s, d1a_ss, d1a_rs, d1b_ss, d1b_rs,
    u1_ss, u1_rs, u2a_ss, u2a_rs, u2b_ss, u2b_rs,
    xs_s, xr_s, ms_s, mr_s, as_s, ar_s, fs_s, fr_s, rs_s, rr_s,
):
    ra, cb = lax.axis_index("ra"), lax.axis_index("cb")
    z, y = lax.div(ra, 4), lax.rem(ra, 4)
    x, c = lax.div(cb, 2), lax.rem(cb, 2)
    far = (4, 3, 5, 2, 6, 1, 7)
    near = (2, 6, 1, 7)
    barrier = pltpu.get_barrier_semaphore()
    loads = [
        pltpu.make_async_copy(src, dst, load_sem.at[k])
        for k, (src, dst) in enumerate(
            [
                (stream_h, stream_v),
                (gain_a, gain_v.at[0]),
                (up_a, up_v.at[0]),
                (down_a, down_v.at[0]),
                (gain_b, gain_v.at[1]),
                (up_b, up_v.at[1]),
                (down_b, down_v.at[1]),
            ]
        )
    ]

    def at(dz, dy, dx, core):
        return {"ra": lax.rem(z + dz, 8) * 4 + lax.rem(y + dy, 4), "cb": lax.rem(x + dx, 4) * 2 + core}

    def send(src, dst, ss, rsem, where):
        pltpu.make_async_remote_copy(
            src_ref=src, dst_ref=dst, send_sem=ss, recv_sem=rsem, device_id=where
        ).start()

    def drain(ref, sem):
        pltpu.make_async_copy(ref, ref, sem).wait()

    def hello(where):
        pl.semaphore_signal(barrier, inc=1, device_id=where)

    def first_up():
        loads[0].wait()
        loads[1].wait()
        u = stream_v[...].astype(F32).T
        loads[2].wait()
        part = nn((u * gain_v[0]).astype(BF), up_v[0].astype(BF))
        ps[:, :, :512] = part.reshape(8, 8, 512).astype(BF)
        return u

    def prepare_up2():
        eye = lax.broadcasted_iota(jnp.int32, (32, 32), 0) == lanes((32, 32))
        column = jnp.sum(jnp.where(eye, gain_v[1], 0.0), axis=1, keepdims=True)
        scaled = (up_v[1].astype(BF).astype(F32) * column).astype(BF)
        for k in range(4):
            up2s[k, c] = scaled[:, 128 * k : 128 * k + 128]

    def prepare_down2():
        down2[c] = down_v[1].astype(BF)

    def finish():
        total = jnp.sum(fr[...].astype(F32), axis=0) + rr[...]
        total = total.astype(BF).astype(F32)
        rolled = pltpu.roll(total, 64, 1)
        out_ref[...] = jnp.concatenate([total, rolled], axis=0)[:, :64].astype(BF)

    for load in loads[:3]:
        load.start()

    @pl.when(c == 0)
    def _():
        for dx in range(4):
            hello(at(0, 0, dx, 1))
        for load in loads[3:]:
            load.start()
        first_up()
        pl.semaphore_wait(barrier, 8)
        for dz in far + (0,):
            send(ps.at[lax.rem(z + dz, 8), :, pl.ds(0, 512)], pr0.at[z], ps_s, pr0_s, at(dz, 0, 0, 1))
        partner = at(0, 0, 0, 1)
        loads[3].wait()
        down1s[...] = down_v[0].astype(BF)
        for dz in near + (0,):
            send(down1s, down1.at[z], d1a_ss, d1a_rs, at(dz, 0, 0, 1))
        loads[4].wait()
        loads[5].wait()
        prepare_up2()
        send(up2s.at[:, 0], up2s.at[:, 0], give_ss.at[0], give_rs.at[0], partner)
        loads[6].wait()
        prepare_down2()
        send(down2.at[0], down2.at[0], give_ss.at[1], give_rs.at[1], partner)
        drain(pr0, ps_s)
        drain(down1.at[pl.ds(0, 5)], d1a_ss)
        drain(up2s.at[:, 0], give_ss.at[0])
        drain(down2.at[0], give_ss.at[1])
        drain(rr, rr_s)
        drain(fr, fr_s)
        finish()

    @pl.when(c == 1)
    def _():
        for dz in far:
            hello(at(dz, 0, 0, 1))
            hello(at(dz, 0, 0, 0))
        for d in (2, 1, 3):
            hello(at(0, d, 0, 1))
            hello(at(0, 0, d, 1))
        hello(at(0, 0, 0, 0))
        for load in loads[3:]:
            load.start()

        u = first_up()
        place = lanes((32, 128)) == 32 * lax.rem(z, 4) + lax.broadcasted_iota(jnp.int32, (32, 128), 0)
        place = place.astype(F32).astype(BF)
        ps[:, :, 512:] = nn(u.astype(BF), place).reshape(8, 8, 128).astype(BF)

        pl.semaphore_wait(barrier, 17)
        for dz in far:
            send(ps.at[lax.rem(z + dz, 8)], pr1.at[z], ps_s, pr1_s, at(dz, 0, 0, 1))
        loads[3].wait()
        down1s[...] = down_v[0].astype(BF)
        for dz in near:
            send(down1s, down1.at[8 + z], d1a_ss, d1a_rs, at(dz, 0, 0, 1))
        pr1[z] = ps[z]
        loads[4].wait()
        loads[5].wait()
        prepare_up2()
        drain(up2s.at[:, 0], give_rs.at[0])
        for dy in (2, 1, 3):
            send(up2s.at[lax.rem(y + dy, 4)], up2y.at[y], u1_ss, u1_rs, at(0, dy, 0, 1))
        up2y[y] = up2s[y]
        down1[8 + z] = down1s[...]

        drain(pr0, pr0_s)
        drain(pr1.at[pl.ds(0, 7)], pr1_s)
        partial = [jnp.sum(pr0[...].astype(F32), axis=0), jnp.sum(pr1[:, :, :512].astype(F32), axis=0)]
        u_own = jnp.concatenate(
            [
                jnp.sum(pr1[0:4, :, 512:].astype(F32), axis=0),
                jnp.sum(pr1[4:8, :, 512:].astype(F32), axis=0),
            ],
            axis=1,
        )
        squares = jnp.sum(u_own * u_own, axis=1, keepdims=True)
        high = squares.astype(BF).astype(F32)
        ys[:, :512] = partial[0].astype(BF)
        ys[:, 512:1024] = partial[1].astype(BF)
        ys[:, 1024:] = jnp.where(lanes((8, 128)) < 64, high, squares - high).astype(BF)
        for dy in (2, 1, 3):
            send(ys, yr.at[y], ys_s, yr_s, at(0, dy, 0, 1))
        yr[y] = ys[...]

        drain(up2y.at[pl.ds(0, 3)], u1_rs)
        for dz in near:
            send(up2y, up2.at[z], u2a_ss, u2a_rs, at(dz, 0, 0, 1))
        up2[z] = up2y[...]

        back, ahead = lax.rem(z + 6, 8), lax.rem(z + 2, 8)
        drain(down1.at[pl.ds(0, 9)], d1a_rs)
        for b, a in ((back, ahead), (back + 8, ahead + 8)):
            send(down1.at[b, pl.ds(0, 16)], down1.at[b, pl.ds(0, 16)], d1b_ss, d1b_rs, at(2, 0, 0, 1))
            send(down1.at[a, pl.ds(16, 16)], down1.at[a, pl.ds(16, 16)], d1b_ss, d1b_rs, at(6, 0, 0, 1))
            send(down1.at[b], down1.at[b], d1b_ss, d1b_rs, at(1, 0, 0, 1))
            send(down1.at[a], down1.at[a], d1b_ss, d1b_rs, at(7, 0, 0, 1))

        drain(yr.at[pl.ds(0, 3)], yr_s)
        preact = jnp.sum(yr[...].astype(F32), axis=0)
        squares = jnp.sum(preact[:, 1024:], axis=1, keepdims=True) / 64
        factor = lax.rsqrt(squares / D + EPS)
        act = jnp.square(jnp.maximum(preact[:, :1024] * factor, 0.0)).astype(BF)

        drain(up2.at[pl.ds(0, 4)], u2a_rs)
        send(up2.at[back, pl.ds(0, 2)], up2.at[back, pl.ds(0, 2)], u2b_ss, u2b_rs, at(2, 0, 0, 1))
        send(up2.at[ahead, pl.ds(2, 2)], up2.at[ahead, pl.ds(2, 2)], u2b_ss, u2b_rs, at(6, 0, 0, 1))
        send(up2.at[back], up2.at[back], u2b_ss, u2b_rs, at(1, 0, 0, 1))
        send(up2.at[ahead], up2.at[ahead], u2b_ss, u2b_rs, at(7, 0, 0, 1))

        drain(down1.at[pl.ds(0, 6)], d1b_rs)
        branch = nt(act[:, :512], down1[:8].reshape(256, 512)) + nt(act[:, 512:], down1[8:].reshape(256, 512))
        share = jnp.where(x == 0, RESIDUAL, 0.0)
        xs[...] = (branch + share * u_own).astype(BF)
        for dy in (2, 1, 3, 0):
            for dx in (2, 1, 3, 0):
                if dy or dx:
                    send(xs, xr.at[4 * y + x], xs_s, xr_s, at(0, dy, dx, 1))
        xr[4 * y + x] = xs[...]
        loads[6].wait()
        prepare_down2()
        drain(down2.at[0], give_rs.at[1])

        drain(xr.at[pl.ds(0, 15)], xr_s)
        middle = jnp.sum(xr[...].astype(F32).reshape(4, 4, 8, 256), axis=1).astype(BF).astype(F32)
        middle = jnp.concatenate([middle[k] for k in range(4)], axis=1)
        squares = jnp.sum(middle * middle, axis=1, keepdims=True)
        factor = lax.rsqrt(squares / D + EPS)
        middle = middle.astype(BF)
        drain(up2.at[pl.ds(0, 3)], u2b_rs)
        pre = []
        for k in range(2):
            rows = jnp.concatenate([up2[a, b, k] for b in range(4) for a in range(8)], axis=0)
            pre.append(nn(middle, rows))
        act = jnp.square(jnp.maximum(jnp.concatenate(pre, axis=1) * factor, 0.0))
        acts[...] = act.astype(BF)

        @pl.loop(1, 32)
        def _(step):
            send(acts, actr.at[8 * y + z], as_s, ar_s, at(lax.div(step, 4), lax.rem(step, 4), 0, 1))

        actr[8 * y + z] = acts[...]
        own = jnp.sum(xr[pl.ds(4 * y, 4)].astype(F32), axis=0).astype(BF)
        ms[0] = own[:, :128]
        ms[1] = own[:, 128:]
        for dz in far:
            send(ms.at[lax.div(lax.rem(z + dz, 8), 4)], mr.at[z], ms_s, mr_s, at(dz, 0, 0, 1))
        mr[z] = ms[lax.div(z, 4)]
        drain(mr.at[pl.ds(0, 7)], mr_s)
        mid = mr[...].astype(F32).reshape(64, 128).astype(BF)
        mid = jnp.concatenate([mid, mid], axis=0)
        rs[...] = RESIDUAL * packed_of(nt(place, mid))
        send(rs, rr, rs_s, rr_s, at(0, 0, 0, 0))
        rr[...] = rs[...]

        drain(actr.at[pl.ds(0, 31)], ar_s)
        weights = jnp.concatenate(
            [down2[k, :, 128 * b : 128 * b + 128] for b in range(4) for k in range(2)], axis=1
        )
        gathered = actr[...].astype(F32).reshape(4, 64, 256)
        gathered = jnp.concatenate([gathered[b] for b in range(4)], axis=1).astype(BF)
        gathered = jnp.concatenate([gathered, gathered], axis=0)
        fs[...] = packed_of(nt(weights, gathered)).astype(BF)
        for dx in (2, 1, 3):
            send(fs, fr.at[x], fs_s, fr_s, at(0, 0, dx, 0))
            send(fs, fr.at[x], fs_s, fr_s, at(0, 0, dx, 1))
        send(fs, fr.at[x], fs_s, fr_s, at(0, 0, 0, 0))
        fr[x] = fs[...]
        drain(fr.at[pl.ds(0, 3)], fr_s)
        finish()

        drain(pr1.at[pl.ds(0, 7)], ps_s)
        drain(down1.at[pl.ds(0, 4)], d1a_ss)
        drain(down1.at[pl.ds(0, 6)], d1b_ss)
        drain(up2y.at[pl.ds(0, 3)], u1_ss)
        drain(yr.at[pl.ds(0, 3)], ys_s)
        drain(up2.at[pl.ds(0, 4)], u2a_ss)
        drain(up2.at[pl.ds(0, 3)], u2b_ss)
        drain(xr.at[pl.ds(0, 15)], xs_s)
        drain(actr.at[pl.ds(0, 31)], as_s)
        drain(mr.at[pl.ds(0, 7)], ms_s)
        drain(rr, rs_s)
        drain(xr.at[pl.ds(0, 7)], fs_s)


def local(stream, gain_first, up_first, down_first, gain_second, up_second, down_second):
    vmem = [
        ((32, 64), BF), ((2, 1, 32), F32), ((2, 32, 512), F32), ((2, 32, 512), F32),
        ((32, 512), BF), ((4, 2, 32, 128), BF), ((2, 32, 512), BF),
        ((8, 8, 640), BF), ((8, 8, 512), BF), ((8, 8, 640), BF), ((8, 1152), BF), ((4, 8, 1152), BF),
        ((16, 32, 512), BF), ((4, 2, 32, 128), BF), ((8, 4, 2, 32, 128), BF),
        ((8, 256), BF), ((16, 8, 256), BF), ((2, 8, 128), BF), ((8, 8, 128), BF),
        ((8, 256), BF), ((32, 8, 256), BF), ((16, 128), BF), ((4, 16, 128), BF),
        ((16, 128), F32), ((16, 128), F32),
    ]
    dma = pltpu.SemaphoreType.DMA
    call = pl.pallas_call(
        kernel,
        out_shape=jax.ShapeDtypeStruct((32, 64), BF),
        in_specs=[pl.BlockSpec(memory_space=pl.ANY)] * 7,
        out_specs=pl.BlockSpec(memory_space=pltpu.VMEM),
        scratch_shapes=[pltpu.VMEM(*v) for v in vmem] + [dma((7,)), dma((2,)), dma((2,))] + [dma(())] * 25,
        compiler_params=pltpu.CompilerParams(collective_id=0, has_side_effects=True),
    )
    out = call(
        stream.T, gain_first[None], up_first, down_first.T, gain_second[None], up_second, down_second.T
    )
    return out.T


def solution(mesh):
    in_specs = (P(None, "ra"), P("ra"), P("ra", "cb"), P("cb", "ra"), P("ra"), P("ra", "cb"), P("cb", "ra"))
    return jax.shard_map(local, mesh=mesh, in_specs=in_specs, out_specs=P(None, "ra"), check_vma=False)
```

time: 37.5 us -> 35.1 us (0.936)
  Pallas kernels: 36 us -> 33.6 us
    pallas_call x1, Pallas kernels: 36 us -> 33.6 us  [local(): call(stream.T, gain_first[None], up_first, down_first.T, gain_second[None...]
where the time goes in v3:
time: 35.1 us; the launch traced here: 34.9 us
  Pallas kernels  33.6 us (96%)
  local copies, waits for them, and re-layouts  1.3 us (4%)
    pallas_call x1, Pallas kernels, local(): call(stream.T, gain_first[None], up_first, down_first.T, gain_second[None...  33.6 us
    unnamed x1, local copies, waits for them, and re-layouts  1.3 us

profile of v3, /device:TPU:1, one launch (start us, length us, event | category | flops | bytes accessed | tf_op | source)
XLA Modules:
  0.0 34.9 jit_solution(13924981003953764448)
XLA Ops:
  0.0 33.6 %shard_map.73 = bf16[32,64]{1,0:T(8,128)(2,1)} custom-call(bf16[32,64]{1,0:T(8,128)(2,1)} %bitcast.9, f32[1,32]{1,0:T(1,128)} %bitcast.10, f32[32,512]{1,0:T(8,128)} %up_a.1, f32[32,512]{1,0:T(8,128)} %bitcast.6, f32[1,32]{1,0:T(1,128)} %bitcast.11, f32[32,512]{1,0:T(8,128)} %up_b.1, f32[32,512]{1,0:T(8,128)} %bitcast.7), custom_call_target="tpu_custom_call" | custom-call | tf_op jit(solution)/shard_map/pallas_call | solution.py:305
  33.6 1.3 %copy.9 = bf16[64,32]{0,1:T(8,128)(2,1)} copy(bf16[64,32]{0,1:T(8,128)(2,1)} %bitcast.8) | data formatting | bytes 8192

commit v4 on v3

--- a/solution.py
+++ b/solution.py
@@ -35,13 +35,12 @@
     ps, pr0, pr1, ys, yr, down1, up2y, up2, xs, xr, ms, mr, acts, actr, fs, fr, rs, rr,
     load_sem, give_ss, give_rs, ps_s, pr0_s, pr1_s, ys_s, yr_s, d1a_ss, d1a_rs, d1b_ss, d1b_rs,
     u1_ss, u1_rs, u2a_ss, u2a_rs, u2b_ss, u2b_rs,
-    xs_s, xr_s, ms_s, mr_s, as_s, ar_s, fs_s, fr_s, rs_s, rr_s,
+    xs_s, xr_s, ms_s, mr_s, as_s, ar_s, fs_s, fr_s, rs_s, rr_s, d1c_ss, d1c_rs, u2c_ss, u2c_rs, go,
 ):
     ra, cb = lax.axis_index("ra"), lax.axis_index("cb")
     z, y = lax.div(ra, 4), lax.rem(ra, 4)
     x, c = lax.div(cb, 2), lax.rem(cb, 2)
     far = (4, 3, 5, 2, 6, 1, 7)
-    near = (2, 6, 1, 7)
     barrier = pltpu.get_barrier_semaphore()
     loads = [
         pltpu.make_async_copy(src, dst, load_sem.at[k])
@@ -83,10 +82,16 @@
 
     def prepare_up2():
         eye = lax.broadcasted_iota(jnp.int32, (32, 32), 0) == lanes((32, 32))
+        loads[4].wait()
+        loads[5].wait()
         column = jnp.sum(jnp.where(eye, gain_v[1], 0.0), axis=1, keepdims=True)
         scaled = (up_v[1].astype(BF).astype(F32) * column).astype(BF)
         for k in range(4):
-            up2s[k, c] = scaled[:, 128 * k : 128 * k + 128]
+            up2s[k] = scaled[:, 128 * k : 128 * k + 128]
+
+    def prepare_down1():
+        loads[3].wait()
+        down1s[...] = down_v[0].astype(BF)
 
     def prepare_down2():
         down2[c] = down_v[1].astype(BF)
@@ -107,25 +112,27 @@
         for load in loads[3:]:
             load.start()
         first_up()
-        pl.semaphore_wait(barrier, 8)
+        prepare_up2()
+        prepare_down1()
+        pl.semaphore_wait(barrier, 1)
+        pl.semaphore_wait(go, 1)
         for dz in far + (0,):
             send(ps.at[lax.rem(z + dz, 8), :, pl.ds(0, 512)], pr0.at[z], ps_s, pr0_s, at(dz, 0, 0, 1))
+        for dy in (2, 1, 3, 0):
+            send(up2s.at[lax.rem(y + dy, 4)], up2y.at[y, 0], u1_ss, u1_rs, at(0, dy, 0, 1))
+        for dz in (2, 6):
+            send(down1s, down1.at[z], d1a_ss, d1a_rs, at(dz, 0, 0, 1))
+        for dz in (1, 7, 0):
+            send(down1s, down1.at[z], d1c_ss, d1c_rs, at(dz, 0, 0, 1))
         partner = at(0, 0, 0, 1)
-        loads[3].wait()
-        down1s[...] = down_v[0].astype(BF)
-        for dz in near + (0,):
-            send(down1s, down1.at[z], d1a_ss, d1a_rs, at(dz, 0, 0, 1))
-        loads[4].wait()
-        loads[5].wait()
-        prepare_up2()
-        send(up2s.at[:, 0], up2s.at[:, 0], give_ss.at[0], give_rs.at[0], partner)
         loads[6].wait()
         prepare_down2()
-        send(down2.at[0], down2.at[0], give_ss.at[1], give_rs.at[1], partner)
+        send(down2.at[0], down2.at[0], give_ss, give_rs, partner)
         drain(pr0, ps_s)
-        drain(down1.at[pl.ds(0, 5)], d1a_ss)
-        drain(up2s.at[:, 0], give_ss.at[0])
-        drain(down2.at[0], give_ss.at[1])
+        drain(down1.at[pl.ds(0, 2)], d1a_ss)
+        drain(down1.at[pl.ds(0, 3)], d1c_ss)
+        drain(up2s, u1_ss)
+        drain(down2.at[0], give_ss)
         drain(rr, rr_s)
         drain(fr, fr_s)
         finish()
@@ -134,7 +141,6 @@
     def _():
         for dz in far:
             hello(at(dz, 0, 0, 1))
-            hello(at(dz, 0, 0, 0))
         for d in (2, 1, 3):
             hello(at(0, d, 0, 1))
             hello(at(0, 0, d, 1))
@@ -146,23 +152,28 @@
         place = lanes((32, 128)) == 32 * lax.rem(z, 4) + lax.broadcasted_iota(jnp.int32, (32, 128), 0)
         place = place.astype(F32).astype(BF)
         ps[:, :, 512:] = nn(u.astype(BF), place).reshape(8, 8, 128).astype(BF)
+        prepare_up2()
+        prepare_down1()
 
         pl.semaphore_wait(barrier, 17)
+        pl.semaphore_signal(go, inc=1, device_id=at(0, 0, 0, 0))
         for dz in far:
             send(ps.at[lax.rem(z + dz, 8)], pr1.at[z], ps_s, pr1_s, at(dz, 0, 0, 1))
-        loads[3].wait()
-        down1s[...] = down_v[0].astype(BF)
-        for dz in near:
+        for dy in (2, 1, 3):
+            send(up2s.at[lax.rem(y + dy, 4)], up2y.at[y, 1], u1_ss, u1_rs, at(0, dy, 0, 1))
+        for dz in (2, 6):
             send(down1s, down1.at[8 + z], d1a_ss, d1a_rs, at(dz, 0, 0, 1))
+        for dz in (1, 7):
+            send(down1s, down1.at[8 + z], d1c_ss, d1c_rs, at(dz, 0, 0, 1))
         pr1[z] = ps[z]
-        loads[4].wait()
-        loads[5].wait()
-        prepare_up2()
-        drain(up2s.at[:, 0], give_rs.at[0])
-        for dy in (2, 1, 3):
-            send(up2s.at[lax.rem(y + dy, 4)], up2y.at[y], u1_ss, u1_rs, at(0, dy, 0, 1))
-        up2y[y] = up2s[y]
         down1[8 + z] = down1s[...]
+        up2y[y, 1] = up2s[y]
+        drain(down1.at[pl.ds(0, 7), :, pl.ds(0, 128)], u1_rs)
+        for dz in (2, 6):
+            send(up2y, up2.at[z], u2a_ss, u2a_rs, at(dz, 0, 0, 1))
+        for dz in (1, 7):
+            send(up2y, up2.at[z], u2c_ss, u2c_rs, at(dz, 0, 0, 1))
+        up2[z] = up2y[...]
 
         drain(pr0, pr0_s)
         drain(pr1.at[pl.ds(0, 7)], pr1_s)
@@ -183,13 +194,8 @@
             send(ys, yr.at[y], ys_s, yr_s, at(0, dy, 0, 1))
         yr[y] = ys[...]
 
-        drain(up2y.at[pl.ds(0, 3)], u1_rs)
-        for dz in near:
-            send(up2y, up2.at[z], u2a_ss, u2a_rs, at(dz, 0, 0, 1))
-        up2[z] = up2y[...]
-
         back, ahead = lax.rem(z + 6, 8), lax.rem(z + 2, 8)
-        drain(down1.at[pl.ds(0, 9)], d1a_rs)
+        drain(down1.at[pl.ds(0, 4)], d1a_rs)
         for b, a in ((back, ahead), (back + 8, ahead + 8)):
             send(down1.at[b, pl.ds(0, 16)], down1.at[b, pl.ds(0, 16)], d1b_ss, d1b_rs, at(2, 0, 0, 1))
             send(down1.at[a, pl.ds(16, 16)], down1.at[a, pl.ds(16, 16)], d1b_ss, d1b_rs, at(6, 0, 0, 1))
@@ -202,12 +208,13 @@
         factor = lax.rsqrt(squares / D + EPS)
         act = jnp.square(jnp.maximum(preact[:, :1024] * factor, 0.0)).astype(BF)
 
-        drain(up2.at[pl.ds(0, 4)], u2a_rs)
+        drain(up2.at[pl.ds(0, 2)], u2a_rs)
         send(up2.at[back, pl.ds(0, 2)], up2.at[back, pl.ds(0, 2)], u2b_ss, u2b_rs, at(2, 0, 0, 1))
         send(up2.at[ahead, pl.ds(2, 2)], up2.at[ahead, pl.ds(2, 2)], u2b_ss, u2b_rs, at(6, 0, 0, 1))
         send(up2.at[back], up2.at[back], u2b_ss, u2b_rs, at(1, 0, 0, 1))
         send(up2.at[ahead], up2.at[ahead], u2b_ss, u2b_rs, at(7, 0, 0, 1))
 
+        drain(down1.at[pl.ds(0, 5)], d1c_rs)
         drain(down1.at[pl.ds(0, 6)], d1b_rs)
         branch = nt(act[:, :512], down1[:8].reshape(256, 512)) + nt(act[:, 512:], down1[8:].reshape(256, 512))
         share = jnp.where(x == 0, RESIDUAL, 0.0)
@@ -219,7 +226,7 @@
         xr[4 * y + x] = xs[...]
         loads[6].wait()
         prepare_down2()
-        drain(down2.at[0], give_rs.at[1])
+        drain(down2.at[0], give_rs)
 
         drain(xr.at[pl.ds(0, 15)], xr_s)
         middle = jnp.sum(xr[...].astype(F32).reshape(4, 4, 8, 256), axis=1).astype(BF).astype(F32)
@@ -227,6 +234,7 @@
         squares = jnp.sum(middle * middle, axis=1, keepdims=True)
         factor = lax.rsqrt(squares / D + EPS)
         middle = middle.astype(BF)
+        drain(up2.at[pl.ds(0, 2)], u2c_rs)
         drain(up2.at[pl.ds(0, 3)], u2b_rs)
         pre = []
         for k in range(2):
@@ -235,9 +243,10 @@
         act = jnp.square(jnp.maximum(jnp.concatenate(pre, axis=1) * factor, 0.0))
         acts[...] = act.astype(BF)
 
-        @pl.loop(1, 32)
-        def _(step):
-            send(acts, actr.at[8 * y + z], as_s, ar_s, at(lax.div(step, 4), lax.rem(step, 4), 0, 1))
+        for k in range(32):
+            @pl.when(ra != k)
+            def _():
+                send(acts, actr.at[8 * y + z], as_s, ar_s, {"ra": k, "cb": cb})
 
         actr[8 * y + z] = acts[...]
         own = jnp.sum(xr[pl.ds(4 * y, 4)].astype(F32), axis=0).astype(BF)
@@ -261,20 +270,24 @@
         gathered = jnp.concatenate([gathered[b] for b in range(4)], axis=1).astype(BF)
         gathered = jnp.concatenate([gathered, gathered], axis=0)
         fs[...] = packed_of(nt(weights, gathered)).astype(BF)
-        for dx in (2, 1, 3):
-            send(fs, fr.at[x], fs_s, fr_s, at(0, 0, dx, 0))
-            send(fs, fr.at[x], fs_s, fr_s, at(0, 0, dx, 1))
-        send(fs, fr.at[x], fs_s, fr_s, at(0, 0, 0, 0))
+        for k in range(4):
+            @pl.when(x != k)
+            def _():
+                send(fs, fr.at[x], fs_s, fr_s, {"ra": ra, "cb": 2 * k + 1})
+        for k in range(4):
+            send(fs, fr.at[x], fs_s, fr_s, {"ra": ra, "cb": 2 * k})
         fr[x] = fs[...]
         drain(fr.at[pl.ds(0, 3)], fr_s)
         finish()
 
         drain(pr1.at[pl.ds(0, 7)], ps_s)
-        drain(down1.at[pl.ds(0, 4)], d1a_ss)
+        drain(down1.at[pl.ds(0, 2)], d1a_ss)
+        drain(down1.at[pl.ds(0, 2)], d1c_ss)
         drain(down1.at[pl.ds(0, 6)], d1b_ss)
-        drain(up2y.at[pl.ds(0, 3)], u1_ss)
+        drain(up2s.at[pl.ds(0, 3)], u1_ss)
         drain(yr.at[pl.ds(0, 3)], ys_s)
-        drain(up2.at[pl.ds(0, 4)], u2a_ss)
+        drain(up2.at[pl.ds(0, 2)], u2a_ss)
+        drain(up2.at[pl.ds(0, 2)], u2c_ss)
         drain(up2.at[pl.ds(0, 3)], u2b_ss)
         drain(xr.at[pl.ds(0, 15)], xs_s)
         drain(actr.at[pl.ds(0, 31)], as_s)
@@ -286,7 +299,7 @@
 def local(stream, gain_first, up_first, down_first, gain_second, up_second, down_second):
     vmem = [
         ((32, 64), BF), ((2, 1, 32), F32), ((2, 32, 512), F32), ((2, 32, 512), F32),
-        ((32, 512), BF), ((4, 2, 32, 128), BF), ((2, 32, 512), BF),
+        ((32, 512), BF), ((4, 32, 128), BF), ((2, 32, 512), BF),
         ((8, 8, 640), BF), ((8, 8, 512), BF), ((8, 8, 640), BF), ((8, 1152), BF), ((4, 8, 1152), BF),
         ((16, 32, 512), BF), ((4, 2, 32, 128), BF), ((8, 4, 2, 32, 128), BF),
         ((8, 256), BF), ((16, 8, 256), BF), ((2, 8, 128), BF), ((8, 8, 128), BF),
@@ -299,7 +312,8 @@
         out_shape=jax.ShapeDtypeStruct((32, 64), BF),
         in_specs=[pl.BlockSpec(memory_space=pl.ANY)] * 7,
         out_specs=pl.BlockSpec(memory_space=pltpu.VMEM),
-        scratch_shapes=[pltpu.VMEM(*v) for v in vmem] + [dma((7,)), dma((2,)), dma((2,))] + [dma(())] * 25,
+        scratch_shapes=[pltpu.VMEM(*v) for v in vmem] + [dma((7,))] + [dma(())] * 31
+        + [pltpu.SemaphoreType.REGULAR],
         compiler_params=pltpu.CompilerParams(collective_id=0, has_side_effects=True),
     )
     out = call(

time: 35.1 us -> 33.8 us (0.963)
  Pallas kernels: 33.6 us -> 32.3 us
    pallas_call x1, Pallas kernels: 33.6 us -> 32.3 us  [local(): call(stream.T, gain_first[None], up_first, down_first.T, gain_second[None...]
where the time goes in v4:
time: 33.8 us; the launch traced here: 33.6 us
  Pallas kernels  32.3 us (96%)
  local copies, waits for them, and re-layouts  1.3 us (4%)
    pallas_call x1, Pallas kernels, local(): call(stream.T, gain_first[None], up_first, down_first.T, gain_second[None...  32.3 us
    unnamed x1, local copies, waits for them, and re-layouts  1.3 us

profile of v4, /device:TPU:1, one launch (start us, length us, event | category | flops | bytes accessed | tf_op | source)
XLA Modules:
  0.0 33.6 jit_solution(6223631617459714332)
XLA Ops:
  0.0 32.3 %shard_map.73 = bf16[32,64]{1,0:T(8,128)(2,1)} custom-call(bf16[32,64]{1,0:T(8,128)(2,1)} %bitcast.9, f32[1,32]{1,0:T(1,128)} %bitcast.10, f32[32,512]{1,0:T(8,128)} %up_a.1, f32[32,512]{1,0:T(8,128)} %bitcast.6, f32[1,32]{1,0:T(1,128)} %bitcast.11, f32[32,512]{1,0:T(8,128)} %up_b.1, f32[32,512]{1,0:T(8,128)} %bitcast.7), custom_call_target="tpu_custom_call" | custom-call | tf_op jit(solution)/shard_map/pallas_call | solution.py:319
  32.3 1.3 %copy.9 = bf16[64,32]{0,1:T(8,128)(2,1)} copy(bf16[64,32]{0,1:T(8,128)(2,1)} %bitcast.8) | data formatting | bytes 8192

commit v5 on v4

--- a/solution.py
+++ b/solution.py
@@ -314,7 +314,7 @@
         out_specs=pl.BlockSpec(memory_space=pltpu.VMEM),
         scratch_shapes=[pltpu.VMEM(*v) for v in vmem] + [dma((7,))] + [dma(())] * 31
         + [pltpu.SemaphoreType.REGULAR],
-        compiler_params=pltpu.CompilerParams(collective_id=0, has_side_effects=True),
+        compiler_params=pltpu.CompilerParams(collective_id=0, has_side_effects=True, vmem_limit_bytes=56535040),
     )
     out = call(
         stream.T, gain_first[None], up_first, down_first.T, gain_second[None], up_second, down_second.T

time: 33.8 us -> 33.1 us (0.979)
  Pallas kernels: 32.3 us -> 31.7 us
    pallas_call x1, Pallas kernels: 32.3 us -> 31.7 us  [local(): call(stream.T, gain_first[None], up_first, down_first.T, gain_second[None...]
    unnamed x1 -> x5, local copies, waits for them, and re-layouts: 1.3 us -> 1.27 us
where the time goes in v5:
time: 33.1 us; the launch traced here: 33 us
  Pallas kernels  31.7 us (96%)
  local copies, waits for them, and re-layouts  1.27 us (4%)
    pallas_call x1, Pallas kernels, local(): call(stream.T, gain_first[None], up_first, down_first.T, gain_second[None...  31.7 us
    unnamed x5, local copies, waits for them, and re-layouts  1.27 us

profile of v5, /device:TPU:1, one launch (start us, length us, event | category | flops | bytes accessed | tf_op | source)
XLA Modules:
  0.0 33.0 jit_solution(5143881841810001878)
XLA Ops:
  0.0 0.0 copy-start
  0.0 0.0 copy-start.1
  0.0 0.7 %copy-done = f32[32]{0:T(128)S(1)} copy-done((f32[32]{0:T(128)S(1)}, f32[32]{0:T(128)}, u32[]{:S(2)}) %copy-start) | copy-done | bytes 152
  0.7 0.0 copy-done.1
  0.7 31.7 %shard_map.73 = bf16[32,64]{1,0:T(8,128)(2,1)S(1)} custom-call(bf16[32,64]{1,0:T(8,128)(2,1)} %bitcast.11, f32[1,32]{1,0:T(1,128)S(1)} %bitcast.7, f32[32,512]{1,0:T(8,128)} %up_a.1, f32[32,512]{1,0:T(8,128)} %bitcast.9, f32[1,32]{1,0:T(1,128)S(1)} %bitcast.8, f32[32,512]{1,0:T(8,128)} %up_b.1, f32[32,512]{1,0:T(8,128)} %bitcast.10), custom_call_target="tpu_custom_call" | custom-call | tf_op jit(solution)/shard_map/pallas_call | solution.py:319
  32.4 0.6 %copy.9 = bf16[64,32]{0,1:T(8,128)(2,1)} copy(bf16[64,32]{0,1:T(8,128)(2,1)S(1)} %bitcast.6) | data formatting | bytes 8192
Async XLA Ops:
  0.0 0.7 %copy-start = (f32[32]{0:T(128)S(1)}, f32[32]{0:T(128)}, u32[]{:S(2)}) copy-start(f32[32]{0:T(128)} %param.8) | copy-start | bytes 388
  0.0 0.7 %copy-start.1 = (f32[32]{0:T(128)S(1)}, f32[32]{0:T(128)}, u32[]{:S(2)}) copy-start(f32[32]{0:T(128)} %param.11) | copy-start | bytes 388

commit v6 on v5

--- a/solution.py
+++ b/solution.py
@@ -24,18 +24,14 @@
     return lax.broadcasted_iota(jnp.int32, shape, len(shape) - 1)
 
 
-def packed_of(both):
-    return jnp.where(lanes((16, 128)) < 64, both[:16], both[16:])
-
-
 def kernel(
     stream_h, gain_a, up_a, down_a, gain_b, up_b, down_b, out_ref,
     stream_v, gain_v, up_v, down_v,
     down1s, up2s, down2,
     ps, pr0, pr1, ys, yr, down1, up2y, up2, xs, xr, ms, mr, acts, actr, fs, fr, rs, rr,
-    load_sem, give_ss, give_rs, ps_s, pr0_s, pr1_s, ys_s, yr_s, d1a_ss, d1a_rs, d1b_ss, d1b_rs,
+    load_sem, fs_s, d1a_rs, give_ss, give_rs, ps_s, pr0_s, pr1_s, ys_s, yr_s, d1a_ss, d1b_ss, d1b_rs,
     u1_ss, u1_rs, u2a_ss, u2a_rs, u2b_ss, u2b_rs,
-    xs_s, xr_s, ms_s, mr_s, as_s, ar_s, fs_s, fr_s, rs_s, rr_s, d1c_ss, d1c_rs, u2c_ss, u2c_rs, go,
+    xs_s, xr_s, ms_s, mr_s, as_s, ar_s, fr_s, rs_s, rr_s, d1c_ss, d1c_rs, u2c_ss, u2c_rs, go,
 ):
     ra, cb = lax.axis_index("ra"), lax.axis_index("cb")
     z, y = lax.div(ra, 4), lax.rem(ra, 4)
@@ -97,16 +93,12 @@
         down2[c] = down_v[1].astype(BF)
 
     def finish():
-        total = jnp.sum(fr[...].astype(F32), axis=0) + rr[...]
-        total = total.astype(BF).astype(F32)
-        rolled = pltpu.roll(total, 64, 1)
-        out_ref[...] = jnp.concatenate([total, rolled], axis=0)[:, :64].astype(BF)
-
-    for load in loads[:3]:
-        load.start()
+        out_ref[...] = (jnp.sum(fr[...].astype(F32), axis=0) + rr[...]).astype(BF)
 
     @pl.when(c == 0)
     def _():
+        for load in loads[:3]:
+            load.start()
         for dx in range(4):
             hello(at(0, 0, dx, 1))
         for load in loads[3:]:
@@ -121,7 +113,7 @@
         for dy in (2, 1, 3, 0):
             send(up2s.at[lax.rem(y + dy, 4)], up2y.at[y, 0], u1_ss, u1_rs, at(0, dy, 0, 1))
         for dz in (2, 6):
-            send(down1s, down1.at[z], d1a_ss, d1a_rs, at(dz, 0, 0, 1))
+            send(down1s, down1.at[z], d1a_ss, d1a_rs.at[0], at(dz, 0, 0, 1))
         for dz in (1, 7, 0):
             send(down1s, down1.at[z], d1c_ss, d1c_rs, at(dz, 0, 0, 1))
         partner = at(0, 0, 0, 1)
@@ -141,6 +133,8 @@
     def _():
         for dz in far:
             hello(at(dz, 0, 0, 1))
+        for load in loads[:3]:
+            load.start()
         for d in (2, 1, 3):
             hello(at(0, d, 0, 1))
             hello(at(0, 0, d, 1))
@@ -162,7 +156,7 @@
         for dy in (2, 1, 3):
             send(up2s.at[lax.rem(y + dy, 4)], up2y.at[y, 1], u1_ss, u1_rs, at(0, dy, 0, 1))
         for dz in (2, 6):
-            send(down1s, down1.at[8 + z], d1a_ss, d1a_rs, at(dz, 0, 0, 1))
+            send(down1s, down1.at[8 + z], d1a_ss, d1a_rs.at[1], at(dz, 0, 0, 1))
         for dz in (1, 7):
             send(down1s, down1.at[8 + z], d1c_ss, d1c_rs, at(dz, 0, 0, 1))
         pr1[z] = ps[z]
@@ -171,9 +165,15 @@
         drain(down1.at[pl.ds(0, 7), :, pl.ds(0, 128)], u1_rs)
         for dz in (2, 6):
             send(up2y, up2.at[z], u2a_ss, u2a_rs, at(dz, 0, 0, 1))
-        for dz in (1, 7):
-            send(up2y, up2.at[z], u2c_ss, u2c_rs, at(dz, 0, 0, 1))
         up2[z] = up2y[...]
+        back, ahead = lax.rem(z + 6, 8), lax.rem(z + 2, 8)
+        drain(down1.at[pl.ds(0, 2)], d1a_rs.at[1])
+        b, a = back + 8, ahead + 8
+        send(down1.at[b, pl.ds(0, 16)], down1.at[b, pl.ds(0, 16)], d1b_ss, d1b_rs, at(2, 0, 0, 1))
+        send(down1.at[a, pl.ds(16, 16)], down1.at[a, pl.ds(16, 16)], d1b_ss, d1b_rs, at(6, 0, 0, 1))
+        send(down1.at[b], down1.at[b], d1b_ss, d1b_rs, at(1, 0, 0, 1))
+        send(down1.at[a], down1.at[a], d1b_ss, d1b_rs, at(7, 0, 0, 1))
+
 
         drain(pr0, pr0_s)
         drain(pr1.at[pl.ds(0, 7)], pr1_s)
@@ -194,14 +194,15 @@
             send(ys, yr.at[y], ys_s, yr_s, at(0, dy, 0, 1))
         yr[y] = ys[...]
 
-        back, ahead = lax.rem(z + 6, 8), lax.rem(z + 2, 8)
-        drain(down1.at[pl.ds(0, 4)], d1a_rs)
-        for b, a in ((back, ahead), (back + 8, ahead + 8)):
-            send(down1.at[b, pl.ds(0, 16)], down1.at[b, pl.ds(0, 16)], d1b_ss, d1b_rs, at(2, 0, 0, 1))
-            send(down1.at[a, pl.ds(16, 16)], down1.at[a, pl.ds(16, 16)], d1b_ss, d1b_rs, at(6, 0, 0, 1))
-            send(down1.at[b], down1.at[b], d1b_ss, d1b_rs, at(1, 0, 0, 1))
-            send(down1.at[a], down1.at[a], d1b_ss, d1b_rs, at(7, 0, 0, 1))
-
+        drain(down1.at[pl.ds(0, 2)], d1a_rs.at[0])
+        b, a = back + 0, ahead + 0
+        send(down1.at[b, pl.ds(0, 16)], down1.at[b, pl.ds(0, 16)], d1b_ss, d1b_rs, at(2, 0, 0, 1))
+        send(down1.at[a, pl.ds(16, 16)], down1.at[a, pl.ds(16, 16)], d1b_ss, d1b_rs, at(6, 0, 0, 1))
+        send(down1.at[b], down1.at[b], d1b_ss, d1b_rs, at(1, 0, 0, 1))
+        send(down1.at[a], down1.at[a], d1b_ss, d1b_rs, at(7, 0, 0, 1))
+
+        for dz in (1, 7):
+            send(up2y, up2.at[z], u2c_ss, u2c_rs, at(dz, 0, 0, 1))
         drain(yr.at[pl.ds(0, 3)], yr_s)
         preact = jnp.sum(yr[...].astype(F32), axis=0)
         squares = jnp.sum(preact[:, 1024:], axis=1, keepdims=True) / 64
@@ -255,12 +256,6 @@
         for dz in far:
             send(ms.at[lax.div(lax.rem(z + dz, 8), 4)], mr.at[z], ms_s, mr_s, at(dz, 0, 0, 1))
         mr[z] = ms[lax.div(z, 4)]
-        drain(mr.at[pl.ds(0, 7)], mr_s)
-        mid = mr[...].astype(F32).reshape(64, 128).astype(BF)
-        mid = jnp.concatenate([mid, mid], axis=0)
-        rs[...] = RESIDUAL * packed_of(nt(place, mid))
-        send(rs, rr, rs_s, rr_s, at(0, 0, 0, 0))
-        rr[...] = rs[...]
 
         drain(actr.at[pl.ds(0, 31)], ar_s)
         weights = jnp.concatenate(
@@ -268,15 +263,19 @@
         )
         gathered = actr[...].astype(F32).reshape(4, 64, 256)
         gathered = jnp.concatenate([gathered[b] for b in range(4)], axis=1).astype(BF)
-        gathered = jnp.concatenate([gathered, gathered], axis=0)
-        fs[...] = packed_of(nt(weights, gathered)).astype(BF)
+        fs[...] = nt(weights, gathered).astype(BF)
         for k in range(4):
             @pl.when(x != k)
             def _():
-                send(fs, fr.at[x], fs_s, fr_s, {"ra": ra, "cb": 2 * k + 1})
+                send(fs, fr.at[x], fs_s.at[1], fr_s, {"ra": ra, "cb": 2 * k + 1})
         for k in range(4):
-            send(fs, fr.at[x], fs_s, fr_s, {"ra": ra, "cb": 2 * k})
+            send(fs, fr.at[x], fs_s.at[0], fr_s, {"ra": ra, "cb": 2 * k})
         fr[x] = fs[...]
+        drain(mr.at[pl.ds(0, 7)], mr_s)
+        mid = mr[...].astype(F32).reshape(64, 128).astype(BF)
+        rs[...] = RESIDUAL * nt(place, mid)
+        send(rs, rr, rs_s, rr_s, at(0, 0, 0, 0))
+        rr[...] = rs[...]
         drain(fr.at[pl.ds(0, 3)], fr_s)
         finish()
 
@@ -293,7 +292,8 @@
         drain(actr.at[pl.ds(0, 31)], as_s)
         drain(mr.at[pl.ds(0, 7)], ms_s)
         drain(rr, rs_s)
-        drain(xr.at[pl.ds(0, 7)], fs_s)
+        drain(fr, fs_s.at[0])
+        drain(fr.at[pl.ds(0, 3)], fs_s.at[1])
 
 
 def local(stream, gain_first, up_first, down_first, gain_second, up_second, down_second):
@@ -303,8 +303,8 @@
         ((8, 8, 640), BF), ((8, 8, 512), BF), ((8, 8, 640), BF), ((8, 1152), BF), ((4, 8, 1152), BF),
         ((16, 32, 512), BF), ((4, 2, 32, 128), BF), ((8, 4, 2, 32, 128), BF),
         ((8, 256), BF), ((16, 8, 256), BF), ((2, 8, 128), BF), ((8, 8, 128), BF),
-        ((8, 256), BF), ((32, 8, 256), BF), ((16, 128), BF), ((4, 16, 128), BF),
-        ((16, 128), F32), ((16, 128), F32),
+        ((8, 256), BF), ((32, 8, 256), BF), ((32, 64), BF), ((4, 32, 64), BF),
+        ((32, 64), F32), ((32, 64), F32),
     ]
     dma = pltpu.SemaphoreType.DMA
     call = pl.pallas_call(
@@ -312,7 +312,7 @@
         out_shape=jax.ShapeDtypeStruct((32, 64), BF),
         in_specs=[pl.BlockSpec(memory_space=pl.ANY)] * 7,
         out_specs=pl.BlockSpec(memory_space=pltpu.VMEM),
-        scratch_shapes=[pltpu.VMEM(*v) for v in vmem] + [dma((7,))] + [dma(())] * 31
+        scratch_shapes=[pltpu.VMEM(*v) for v in vmem] + [dma((7,)), dma((2,)), dma((2,))] + [dma(())] * 29
         + [pltpu.SemaphoreType.REGULAR],
         compiler_params=pltpu.CompilerParams(collective_id=0, has_side_effects=True, vmem_limit_bytes=56535040),
     )

time: 33.1 us -> 32.7 us (0.988)
  Pallas kernels: 31.7 us -> 31.3 us
    pallas_call x1, Pallas kernels: 31.7 us -> 31.3 us  [local(): call(stream.T, gain_first[None], up_first, down_first.T, gain_second[None...]
where the time goes in v6:
time: 32.7 us; the launch traced here: 32.6 us
  Pallas kernels  31.3 us (96%)
  local copies, waits for them, and re-layouts  1.27 us (4%)
    pallas_call x1, Pallas kernels, local(): call(stream.T, gain_first[None], up_first, down_first.T, gain_second[None...  31.3 us
    unnamed x5, local copies, waits for them, and re-layouts  1.27 us

profile of v6, /device:TPU:1, one launch (start us, length us, event | category | flops | bytes accessed | tf_op | source)
XLA Modules:
  0.0 32.6 jit_solution(895710118656151840)
XLA Ops:
  0.0 0.0 copy-start
  0.0 0.0 copy-start.1
  0.0 0.7 %copy-done = f32[32]{0:T(128)S(1)} copy-done((f32[32]{0:T(128)S(1)}, f32[32]{0:T(128)}, u32[]{:S(2)}) %copy-start) | copy-done | bytes 152
  0.7 0.0 copy-done.1
  0.7 31.3 %shard_map.73 = bf16[32,64]{1,0:T(8,128)(2,1)S(1)} custom-call(bf16[32,64]{1,0:T(8,128)(2,1)} %bitcast.11, f32[1,32]{1,0:T(1,128)S(1)} %bitcast.7, f32[32,512]{1,0:T(8,128)} %up_a.1, f32[32,512]{1,0:T(8,128)} %bitcast.9, f32[1,32]{1,0:T(1,128)S(1)} %bitcast.8, f32[32,512]{1,0:T(8,128)} %up_b.1, f32[32,512]{1,0:T(8,128)} %bitcast.10), custom_call_target="tpu_custom_call" | custom-call | tf_op jit(solution)/shard_map/pallas_call | solution.py:319
  32.0 0.6 %copy.9 = bf16[64,32]{0,1:T(8,128)(2,1)} copy(bf16[64,32]{0,1:T(8,128)(2,1)S(1)} %bitcast.6) | data formatting | bytes 8192
Async XLA Ops:
  0.0 0.7 %copy-start = (f32[32]{0:T(128)S(1)}, f32[32]{0:T(128)}, u32[]{:S(2)}) copy-start(f32[32]{0:T(128)} %param.8) | copy-start | bytes 388
  0.0 0.7 %copy-start.1 = (f32[32]{0:T(128)S(1)}, f32[32]{0:T(128)}, u32[]{:S(2)}) copy-start(f32[32]{0:T(128)} %param.11) | copy-start | bytes 388

commit v7 on v6

--- a/solution.py
+++ b/solution.py
@@ -108,10 +108,10 @@
         prepare_down1()
         pl.semaphore_wait(barrier, 1)
         pl.semaphore_wait(go, 1)
+        for dy in (2, 1, 3, 0):
+            send(up2s.at[lax.rem(y + dy, 4)], up2y.at[y, 0], u1_ss, u1_rs, at(0, dy, 0, 1))
         for dz in far + (0,):
             send(ps.at[lax.rem(z + dz, 8), :, pl.ds(0, 512)], pr0.at[z], ps_s, pr0_s, at(dz, 0, 0, 1))
-        for dy in (2, 1, 3, 0):
-            send(up2s.at[lax.rem(y + dy, 4)], up2y.at[y, 0], u1_ss, u1_rs, at(0, dy, 0, 1))
         for dz in (2, 6):
             send(down1s, down1.at[z], d1a_ss, d1a_rs.at[0], at(dz, 0, 0, 1))
         for dz in (1, 7, 0):
@@ -151,12 +151,12 @@
 
         pl.semaphore_wait(barrier, 17)
         pl.semaphore_signal(go, inc=1, device_id=at(0, 0, 0, 0))
-        for dz in far:
-            send(ps.at[lax.rem(z + dz, 8)], pr1.at[z], ps_s, pr1_s, at(dz, 0, 0, 1))
         for dy in (2, 1, 3):
             send(up2s.at[lax.rem(y + dy, 4)], up2y.at[y, 1], u1_ss, u1_rs, at(0, dy, 0, 1))
         for dz in (2, 6):
             send(down1s, down1.at[8 + z], d1a_ss, d1a_rs.at[1], at(dz, 0, 0, 1))
+        for dz in far:
+            send(ps.at[lax.rem(z + dz, 8)], pr1.at[z], ps_s, pr1_s, at(dz, 0, 0, 1))
         for dz in (1, 7):
             send(down1s, down1.at[8 + z], d1c_ss, d1c_rs, at(dz, 0, 0, 1))
         pr1[z] = ps[z]
@@ -244,10 +244,18 @@
         act = jnp.square(jnp.maximum(jnp.concatenate(pre, axis=1) * factor, 0.0))
         acts[...] = act.astype(BF)
 
-        for k in range(32):
-            @pl.when(ra != k)
-            def _():
-                send(acts, actr.at[8 * y + z], as_s, ar_s, {"ra": k, "cb": cb})
+        @pl.when(ra != 0)
+        def _():
+            send(acts, actr.at[8 * y + z], as_s, ar_s, {"ra": 0, "cb": cb})
+
+        for dz in far + (0,):
+            for dy in (2, 1, 3, 0):
+                if dz or dy:
+                    other = at(dz, dy, 0, 1)
+
+                    @pl.when(other["ra"] != 0)
+                    def _():
+                        send(acts, actr.at[8 * y + z], as_s, ar_s, other)
 
         actr[8 * y + z] = acts[...]
         own = jnp.sum(xr[pl.ds(4 * y, 4)].astype(F32), axis=0).astype(BF)

time: 32.7 us -> 32.4 us (level)
    pallas_call x1, Pallas kernels: 31.3 us -> 31 us  [local(): call(stream.T, gain_first[None], up_first, down_first.T, gain_second[None...]
where the time goes in v7:
time: 32.4 us; the launch traced here: 32.3 us
  Pallas kernels  31 us (96%)
  local copies, waits for them, and re-layouts  1.27 us (4%)
    pallas_call x1, Pallas kernels, local(): call(stream.T, gain_first[None], up_first, down_first.T, gain_second[None...  31 us
    unnamed x5, local copies, waits for them, and re-layouts  1.27 us

profile of v7, /device:TPU:1, one launch (start us, length us, event | category | flops | bytes accessed | tf_op | source)
XLA Modules:
  0.0 32.3 jit_solution(940468107489947519)
XLA Ops:
  0.0 0.0 copy-start
  0.0 0.0 copy-start.1
  0.0 0.7 %copy-done = f32[32]{0:T(128)S(1)} copy-done((f32[32]{0:T(128)S(1)}, f32[32]{0:T(128)}, u32[]{:S(2)}) %copy-start) | copy-done | bytes 152
  0.7 0.0 copy-done.1
  0.7 31.0 %shard_map.73 = bf16[32,64]{1,0:T(8,128)(2,1)S(1)} custom-call(bf16[32,64]{1,0:T(8,128)(2,1)} %bitcast.11, f32[1,32]{1,0:T(1,128)S(1)} %bitcast.7, f32[32,512]{1,0:T(8,128)} %up_a.1, f32[32,512]{1,0:T(8,128)} %bitcast.9, f32[1,32]{1,0:T(1,128)S(1)} %bitcast.8, f32[32,512]{1,0:T(8,128)} %up_b.1, f32[32,512]{1,0:T(8,128)} %bitcast.10), custom_call_target="tpu_custom_call" | custom-call | tf_op jit(solution)/shard_map/pallas_call | solution.py:327
  31.7 0.6 %copy.9 = bf16[64,32]{0,1:T(8,128)(2,1)} copy(bf16[64,32]{0,1:T(8,128)(2,1)S(1)} %bitcast.6) | data formatting | bytes 8192
Async XLA Ops:
  0.0 0.7 %copy-start = (f32[32]{0:T(128)S(1)}, f32[32]{0:T(128)}, u32[]{:S(2)}) copy-start(f32[32]{0:T(128)} %param.8) | copy-start | bytes 388
  0.0 0.7 %copy-start.1 = (f32[32]{0:T(128)S(1)}, f32[32]{0:T(128)}, u32[]{:S(2)}) copy-start(f32[32]{0:T(128)} %param.11) | copy-start | bytes 388

commit v8 on v7

--- a/solution.py
+++ b/solution.py
@@ -190,16 +190,16 @@
         ys[:, :512] = partial[0].astype(BF)
         ys[:, 512:1024] = partial[1].astype(BF)
         ys[:, 1024:] = jnp.where(lanes((8, 128)) < 64, high, squares - high).astype(BF)
-        for dy in (2, 1, 3):
-            send(ys, yr.at[y], ys_s, yr_s, at(0, dy, 0, 1))
-        yr[y] = ys[...]
-
         drain(down1.at[pl.ds(0, 2)], d1a_rs.at[0])
         b, a = back + 0, ahead + 0
         send(down1.at[b, pl.ds(0, 16)], down1.at[b, pl.ds(0, 16)], d1b_ss, d1b_rs, at(2, 0, 0, 1))
         send(down1.at[a, pl.ds(16, 16)], down1.at[a, pl.ds(16, 16)], d1b_ss, d1b_rs, at(6, 0, 0, 1))
         send(down1.at[b], down1.at[b], d1b_ss, d1b_rs, at(1, 0, 0, 1))
         send(down1.at[a], down1.at[a], d1b_ss, d1b_rs, at(7, 0, 0, 1))
+
+        for dy in (2, 1, 3):
+            send(ys, yr.at[y], ys_s, yr_s, at(0, dy, 0, 1))
+        yr[y] = ys[...]
 
         for dz in (1, 7):
             send(up2y, up2.at[z], u2c_ss, u2c_rs, at(dz, 0, 0, 1))
@@ -265,12 +265,12 @@
             send(ms.at[lax.div(lax.rem(z + dz, 8), 4)], mr.at[z], ms_s, mr_s, at(dz, 0, 0, 1))
         mr[z] = ms[lax.div(z, 4)]
 
-        drain(actr.at[pl.ds(0, 31)], ar_s)
         weights = jnp.concatenate(
             [down2[k, :, 128 * b : 128 * b + 128] for b in range(4) for k in range(2)], axis=1
         )
-        gathered = actr[...].astype(F32).reshape(4, 64, 256)
-        gathered = jnp.concatenate([gathered[b] for b in range(4)], axis=1).astype(BF)
+        drain(actr.at[pl.ds(0, 31)], ar_s)
+        gathered = actr[...].reshape(4, 64, 256)
+        gathered = jnp.concatenate([gathered[b] for b in range(4)], axis=1)
         fs[...] = nt(weights, gathered).astype(BF)
         for k in range(4):
             @pl.when(x != k)

time: 32.4 us -> 32.5 us (level)
  no operation moved by 1% of the time
where the time goes in v8:
time: 32.5 us; the launch traced here: 32.3 us
  Pallas kernels  31 us (95%)
  local copies, waits for them, and re-layouts  1.27 us (4%)
    pallas_call x1, Pallas kernels, local(): call(stream.T, gain_first[None], up_first, down_first.T, gain_second[None...  31 us
    unnamed x5, local copies, waits for them, and re-layouts  1.27 us

profile of v8, /device:TPU:1, one launch (start us, length us, event | category | flops | bytes accessed | tf_op | source)
XLA Modules:
  0.0 32.3 jit_solution(190575519279024869)
XLA Ops:
  0.0 0.0 copy-start
  0.0 0.0 copy-start.1
  0.0 0.7 %copy-done = f32[32]{0:T(128)S(1)} copy-done((f32[32]{0:T(128)S(1)}, f32[32]{0:T(128)}, u32[]{:S(2)}) %copy-start) | copy-done | bytes 152
  0.7 0.0 copy-done.1
  0.7 31.0 %shard_map.73 = bf16[32,64]{1,0:T(8,128)(2,1)S(1)} custom-call(bf16[32,64]{1,0:T(8,128)(2,1)} %bitcast.11, f32[1,32]{1,0:T(1,128)S(1)} %bitcast.7, f32[32,512]{1,0:T(8,128)} %up_a.1, f32[32,512]{1,0:T(8,128)} %bitcast.9, f32[1,32]{1,0:T(1,128)S(1)} %bitcast.8, f32[32,512]{1,0:T(8,128)} %up_b.1, f32[32,512]{1,0:T(8,128)} %bitcast.10), custom_call_target="tpu_custom_call" | custom-call | tf_op jit(solution)/shard_map/pallas_call | solution.py:327
  31.7 0.6 %copy.9 = bf16[64,32]{0,1:T(8,128)(2,1)} copy(bf16[64,32]{0,1:T(8,128)(2,1)S(1)} %bitcast.6) | data formatting | bytes 8192
Async XLA Ops:
  0.0 0.7 %copy-start = (f32[32]{0:T(128)S(1)}, f32[32]{0:T(128)}, u32[]{:S(2)}) copy-start(f32[32]{0:T(128)} %param.8) | copy-start | bytes 388
  0.0 0.7 %copy-start.1 = (f32[32]{0:T(128)S(1)}, f32[32]{0:T(128)}, u32[]{:S(2)}) copy-start(f32[32]{0:T(128)} %param.11) | copy-start | bytes 388

commit v9 on v8

--- a/solution.py
+++ b/solution.py
@@ -322,7 +322,7 @@
         out_specs=pl.BlockSpec(memory_space=pltpu.VMEM),
         scratch_shapes=[pltpu.VMEM(*v) for v in vmem] + [dma((7,)), dma((2,)), dma((2,))] + [dma(())] * 29
         + [pltpu.SemaphoreType.REGULAR],
-        compiler_params=pltpu.CompilerParams(collective_id=0, has_side_effects=True, vmem_limit_bytes=56535040),
+        compiler_params=pltpu.CompilerParams(collective_id=0, has_side_effects=True, vmem_limit_bytes=56528896),
     )
     out = call(
         stream.T, gain_first[None], up_first, down_first.T, gain_second[None], up_second, down_second.T

time: 32.5 us -> 32.5 us (level)
    unnamed x5 -> x7, local copies, waits for them, and re-layouts: 1.27 us -> 1.3 us
where the time goes in v9:
time: 32.5 us; the launch traced here: 32.3 us
  Pallas kernels  31 us (95%)
  local copies, waits for them, and re-layouts  1.3 us (4%)
    pallas_call x1, Pallas kernels, local(): call(stream.T, gain_first[None], up_first, down_first.T, gain_second[None...  31 us
    unnamed x7, local copies, waits for them, and re-layouts  1.3 us

profile of v9, /device:TPU:1, one launch (start us, length us, event | category | flops | bytes accessed | tf_op | source)
XLA Modules:
  0.0 32.3 jit_solution(9050105951958145390)
XLA Ops:
  0.0 0.0 copy-start
  0.0 0.0 copy-start.1
  0.0 0.0 copy-start.2
  0.0 0.7 %copy-done = bf16[64,32]{0,1:T(8,128)(2,1)S(1)} copy-done((bf16[64,32]{0,1:T(8,128)(2,1)S(1)}, bf16[64,32]{0,1:T(8,128)(2,1)}, u32[]{:S(2)}) %copy-start) | copy-done | bytes 4120
  0.7 0.0 copy-done.1
  0.7 0.0 copy-done.2
  0.7 31.0 %shard_map.73 = bf16[32,64]{1,0:T(8,128)(2,1)S(1)} custom-call(bf16[32,64]{1,0:T(8,128)(2,1)S(1)} %bitcast.7, f32[1,32]{1,0:T(1,128)S(1)} %bitcast.8, f32[32,512]{1,0:T(8,128)} %up_a.1, f32[32,512]{1,0:T(8,128)} %bitcast.10, f32[1,32]{1,0:T(1,128)S(1)} %bitcast.9, f32[32,512]{1,0:T(8,128)} %up_b.1, f32[32,512]{1,0:T(8,128)} %bitcast.11), custom_call_target="tpu_custom_call" | custom-call | tf_op jit(solution)/shard_map/pallas_call | solution.py:327
  31.7 0.6 %copy.9 = bf16[64,32]{0,1:T(8,128)(2,1)} copy(bf16[64,32]{0,1:T(8,128)(2,1)S(1)} %bitcast.6) | data formatting | bytes 8192
Async XLA Ops:
  0.0 0.7 %copy-start = (bf16[64,32]{0,1:T(8,128)(2,1)S(1)}, bf16[64,32]{0,1:T(8,128)(2,1)}, u32[]{:S(2)}) copy-start(bf16[64,32]{0,1:T(8,128)(2,1)} %param.7) | copy-start | bytes 12292
  0.0 0.7 %copy-start.1 = (f32[32]{0:T(128)S(1)}, f32[32]{0:T(128)}, u32[]{:S(2)}) copy-start(f32[32]{0:T(128)} %param.8) | copy-start | bytes 388
  0.0 0.7 %copy-start.2 = (f32[32]{0:T(128)S(1)}, f32[32]{0:T(128)}, u32[]{:S(2)}) copy-start(f32[32]{0:T(128)} %param.11) | copy-start | bytes 388

commit v10 on v8

--- a/solution.py
+++ b/solution.py
@@ -155,7 +155,7 @@
             send(up2s.at[lax.rem(y + dy, 4)], up2y.at[y, 1], u1_ss, u1_rs, at(0, dy, 0, 1))
         for dz in (2, 6):
             send(down1s, down1.at[8 + z], d1a_ss, d1a_rs.at[1], at(dz, 0, 0, 1))
-        for dz in far:
+        for dz in (4, 5, 3, 6, 2, 7, 1):
             send(ps.at[lax.rem(z + dz, 8)], pr1.at[z], ps_s, pr1_s, at(dz, 0, 0, 1))
         for dz in (1, 7):
             send(down1s, down1.at[8 + z], d1c_ss, d1c_rs, at(dz, 0, 0, 1))

time: 32.5 us -> 32.5 us (level)
  no operation moved by 1% of the time
where the time goes in v10:
time: 32.5 us; the launch traced here: 32.3 us
  Pallas kernels  31 us (95%)
  local copies, waits for them, and re-layouts  1.27 us (4%)
    pallas_call x1, Pallas kernels, local(): call(stream.T, gain_first[None], up_first, down_first.T, gain_second[None...  31 us
    unnamed x5, local copies, waits for them, and re-layouts  1.27 us

profile of v10, /device:TPU:1, one launch (start us, length us, event | category | flops | bytes accessed | tf_op | source)
XLA Modules:
  0.0 32.3 jit_solution(62586897195400641)
XLA Ops:
  0.0 0.0 copy-start
  0.0 0.0 copy-start.1
  0.0 0.7 %copy-done = f32[32]{0:T(128)S(1)} copy-done((f32[32]{0:T(128)S(1)}, f32[32]{0:T(128)}, u32[]{:S(2)}) %copy-start) | copy-done | bytes 152
  0.7 0.0 copy-done.1
  0.7 31.0 %shard_map.73 = bf16[32,64]{1,0:T(8,128)(2,1)S(1)} custom-call(bf16[32,64]{1,0:T(8,128)(2,1)} %bitcast.11, f32[1,32]{1,0:T(1,128)S(1)} %bitcast.7, f32[32,512]{1,0:T(8,128)} %up_a.1, f32[32,512]{1,0:T(8,128)} %bitcast.9, f32[1,32]{1,0:T(1,128)S(1)} %bitcast.8, f32[32,512]{1,0:T(8,128)} %up_b.1, f32[32,512]{1,0:T(8,128)} %bitcast.10), custom_call_target="tpu_custom_call" | custom-call | tf_op jit(solution)/shard_map/pallas_call | solution.py:327
  31.7 0.6 %copy.9 = bf16[64,32]{0,1:T(8,128)(2,1)} copy(bf16[64,32]{0,1:T(8,128)(2,1)S(1)} %bitcast.6) | data formatting | bytes 8192
Async XLA Ops:
  0.0 0.7 %copy-start = (f32[32]{0:T(128)S(1)}, f32[32]{0:T(128)}, u32[]{:S(2)}) copy-start(f32[32]{0:T(128)} %param.8) | copy-start | bytes 388
  0.0 0.7 %copy-start.1 = (f32[32]{0:T(128)S(1)}, f32[32]{0:T(128)}, u32[]{:S(2)}) copy-start(f32[32]{0:T(128)} %param.11) | copy-start | bytes 388
